TPU v7x, 32 devices: a whole 2x2x4 slice. The times are simulated.
32 devices in a mesh: grp: 2 (over x), ep: 16 (over z, y, core).
Axes of the slice: x: 2, y: 2, z: 4, core: 2. Of those that a mesh axis runs over, the one named last changes fastest.
Arguments:
- tokens: bfloat16 [128, 2048], P(('grp', 'ep')), parts along dimension 0, may hold values from -30 to 30
- state: float32 [128, 16, 128, 128], P(('grp', 'ep')), parts along dimension 0, may hold values from -6 to 6
- route_ids: int32 [128, 2], P(('grp', 'ep')), parts along dimension 0, may hold values from 0 to 3, all different within a row; in each aligned block of 4 rows (0 to 3, 4 to 7, ...) at most 3 rows name the same one
- route_weights: bfloat16 [128, 2], P(('grp', 'ep')), parts along dimension 0, may hold values from 0.099609375 to 1
- norm_mix: float32 [2048], replicated, may hold values from 0.1 to 1.9
- w_query: bfloat16 [2048, 2048], P(None, 'ep'), may hold values from -0.125 to 0.125
- w_forget: bfloat16 [2048, 2048], P(None, 'ep'), may hold values from -0.125 to 0.125
- w_input: bfloat16 [2048, 2048], P(None, 'ep'), may hold values from -0.125 to 0.125
- w_gate: bfloat16 [2048, 2048], P(None, 'ep'), may hold values from -0.125 to 0.125
- lower_bound: float32 [2048], replicated, may hold values from 0.05 to 0.9
- head_gain: float32 [128], replicated, may hold values from 0.1 to 1.9
- w_out: bfloat16 [2048, 2048], P(None, 'ep'), may hold values from -0.125 to 0.125
- norm_ffn: float32 [2048], replicated, may hold values from 0.1 to 1.9
- expert_gate: bfloat16 [2048, 28672], P(None, 'ep'), may hold values from -0.125 to 0.125
- expert_up: bfloat16 [2048, 28672], P(None, 'ep'), may hold values from -0.125 to 0.125
- expert_down: bfloat16 [28672, 2048], P('ep'), may hold values from -0.0625 to 0.0625
Outputs:
- layer_out: bfloat16 [128, 2048], P(('grp', 'ep')), parts along dimension 0
- new_state: float32 [128, 16, 128, 128], P(('grp', 'ep')), parts along dimension 0
There are 2 independent parts, one for each index of `grp`. A program takes and returns all parts, laid end to end along the dimension named above; an argument that names none is the same for every part. Nothing has to cross between parts.
Inputs may be any that keep to these rules, and one draw needn't show every extreme that they name: `route_ids`: each row names 2 different experts; the rows of one device name no expert more than 3 times, and some device names one exactly 3 times.
All inputs are finite; a program needn't handle non-finite values.
Results may differ from a plain program's by a relative error of at most 0.008.
Values may be sent and summed in bfloat16 or wider, within the bound.
No kernel may reach another device: no remote copies, remote signals or barrier semaphores. Data moves between devices by JAX's collectives and lax.ppermute only.
A program may use at most 64 MiB of HBM per device.

v0:
```python
import jax
import jax.numpy as jnp
from jax import lax
from jax.sharding import PartitionSpec as P

FF = 7168
EXPERTS = 4
CAP = 3


epsilon = 1e-06


def rms_scale(values, gain):
    return values * lax.rsqrt(jnp.mean(values * values, axis=-1, keepdims=True) + epsilon) * gain


def mixer_state(projected, state, lower_bound, head_gain):
    query_raw = projected[0].astype(jnp.float32)
    forget_raw = projected[1].astype(jnp.float32)
    input_raw = projected[2].astype(jnp.float32)
    gate_raw = projected[3].astype(jnp.float32)
    seq_rows = state.shape[0]
    heads = state.shape[1]
    head_dim = state.shape[2]
    head_shape = (seq_rows, heads, head_dim)
    log_forget = jnp.logaddexp(
        jnp.log(lower_bound), jnp.log1p(-lower_bound) + jax.nn.log_sigmoid(forget_raw)
    )
    key_vec = (1.0 - lower_bound) * jax.nn.sigmoid(-forget_raw)
    query_vec = jax.nn.silu(query_raw) * head_dim ** (-0.5)
    new_state = (
        jnp.exp(log_forget).reshape(head_shape)[..., None] * state
        + key_vec.reshape(head_shape)[..., None] * input_raw.reshape(head_shape)[:, :, None, :]
    )
    read_out = jnp.einsum(
        "thk,thkv->thv", query_vec.reshape(head_shape), new_state, precision=lax.Precision.HIGHEST
    )
    mixed = rms_scale(read_out, head_gain) * jax.nn.silu(gate_raw.reshape(head_shape))
    return (mixed.reshape(seq_rows, heads * head_dim).astype(jnp.bfloat16), new_state)


def local(
    tokens,
    state,
    route_ids,
    route_weights,
    norm_mix,
    w_query,
    w_forget,
    w_input,
    w_gate,
    lower_bound,
    head_gain,
    w_out,
    norm_ffn,
    expert_gate,
    expert_up,
    expert_down,
):
    model_width = tokens.shape[1]
    expert_group = FF // expert_gate.shape[1]
    all_tokens, all_ids, all_weights = (
        lax.all_gather(tokens, "ep", axis=0, tiled=True),
        lax.all_gather(route_ids, "ep", axis=0, tiled=True),
        lax.all_gather(route_weights, "ep", axis=0, tiled=True),
    )
    normed = rms_scale(all_tokens.astype(jnp.float32), norm_mix).astype(jnp.bfloat16)
    projected = jnp.stack(
        [
            jnp.dot(normed, weight, preferred_element_type=jnp.float32).astype(jnp.bfloat16)
            for weight in (w_query, w_forget, w_input, w_gate)
        ]
    )
    owned = lax.all_to_all(projected, "ep", split_axis=1, concat_axis=2, tiled=True)
    mixed, new_state = mixer_state(owned, state, lower_bound, head_gain)
    mixer_cols = jnp.dot(
        lax.all_gather(mixed, "ep", axis=0, tiled=True), w_out, preferred_element_type=jnp.float32
    ).astype(jnp.bfloat16)
    mixer_rows = lax.all_to_all(mixer_cols, "ep", split_axis=0, concat_axis=1, tiled=True)
    middle = tokens.astype(jnp.float32) + mixer_rows.astype(jnp.float32)
    normed_two = rms_scale(middle, norm_ffn).astype(jnp.bfloat16)
    matches = (route_ids[:, :, None] == jnp.arange(EXPERTS, dtype=jnp.int32)[None, None, :]).astype(
        jnp.int32
    )
    hit_mask = jnp.sum(matches, axis=1)
    combined = jnp.sum(
        route_weights.astype(jnp.float32)[:, :, None] * matches.astype(jnp.float32), axis=1
    )
    slot_rank = jnp.cumsum(hit_mask, axis=0) - hit_mask
    slot_ids = jnp.arange(CAP, dtype=jnp.int32)
    placing = (
        (slot_rank.T[:, None, :] == slot_ids[None, :, None]) & (hit_mask.T[:, None, :] > 0)
    ).astype(jnp.float32)
    outgoing = jnp.einsum(
        "ect,td->ecd", placing.astype(jnp.bfloat16), normed_two, preferred_element_type=jnp.float32
    ).astype(jnp.bfloat16)
    outgoing = jnp.repeat(outgoing, expert_group, axis=0)
    arrived = lax.all_to_all(outgoing, "ep", split_axis=0, concat_axis=0, tiled=True)
    gate_act = jnp.einsum("scd,df->scf", arrived, expert_gate, preferred_element_type=jnp.float32)
    up_act = jnp.einsum("scd,df->scf", arrived, expert_up, preferred_element_type=jnp.float32)
    hidden = (jax.nn.silu(gate_act) * up_act).astype(jnp.bfloat16)
    partial_rows = jnp.einsum(
        "scf,fd->scd", hidden, expert_down, preferred_element_type=jnp.float32
    )
    returned = lax.all_to_all(
        partial_rows.astype(jnp.bfloat16), "ep", split_axis=0, concat_axis=0, tiled=True
    ).astype(partial_rows.dtype)
    summed = jnp.sum(
        returned.reshape(EXPERTS, expert_group, returned.shape[1], model_width), axis=1
    )
    expert_total = jnp.einsum(
        "ect,ecd->td", placing * combined.T[:, None, :], summed, precision=lax.Precision.HIGHEST
    )
    layer_out = (middle + expert_total).astype(jnp.bfloat16)
    return (layer_out, new_state)


def solution(mesh):
    return jax.shard_map(
        local,
        mesh=mesh,
        in_specs=(
            P(("grp", "ep"), None),
            P(("grp", "ep"), None, None, None),
            P(("grp", "ep"), None),
            P(("grp", "ep"), None),
            P(),
            P(None, "ep"),
            P(None, "ep"),
            P(None, "ep"),
            P(None, "ep"),
            P(),
            P(),
            P(None, "ep"),
            P(),
            P(None, "ep"),
            P(None, "ep"),
            P("ep", None),
        ),
        out_specs=(P(("grp", "ep"), None), P(("grp", "ep"), None, None, None)),
        check_vma=False,
    )
```

profile of v0, /device:TPU:0, one launch (start us, length us, event | category | flops | bytes accessed | tf_op | source)
XLA Modules:
  0.0 121.8 jit_solution(15939425539012757206)
XLA Ops:
  0.6 24.2 %all-gather = bf16[16,4,2048]{2,1,0:T(4,128)(2,1)S(1)} all-gather(bf16[1,4,2048]{2,1,0:T(4,128)(2,1)} %bitcast.138), channel_id=1, replica_groups=mesh['grp'=2,'ep'=16] {'ep'}, dimensions={0}, use_global_device_ids=true | all-gather | bytes 278528 | tf_op jit(solution)/shard_map/all_gather | solution.py:64
  24.9 0.1 multiply_reduce_fusion
  25.0 0.8 multiply_convert_fusion
  25.9 0.2 fusion.17
  26.1 1.3 %fusion.18 = bf16[1,64,128]{2,1,0:T(8,128)(2,1)S(1)} fusion(bf16[64,2048]{1,0:T(8,128)(2,1)S(1)} %multiply_convert_fusion, bf16[2048,128]{1,0:T(8,128)(2,1)} %param.22), kind=kOutput, calls=%fused_computation.20 | convolution fusion | flops 33562624 | bytes 802816 | tf_op jit(solution)/shard_map/dot_general | solution.py:71
  27.4 1.3 %fusion.19 = bf16[1,64,128]{2,1,0:T(8,128)(2,1)S(1)} fusion(bf16[64,2048]{1,0:T(8,128)(2,1)S(1)} %multiply_convert_fusion, bf16[2048,128]{1,0:T(8,128)(2,1)} %param.23), kind=kOutput, calls=%fused_computation.21 | convolution fusion | flops 33562624 | bytes 802816 | tf_op jit(solution)/shard_map/dot_general | solution.py:71
  28.7 1.3 %fusion.20 = bf16[1,64,128]{2,1,0:T(8,128)(2,1)S(1)} fusion(bf16[64,2048]{1,0:T(8,128)(2,1)S(1)} %multiply_convert_fusion, bf16[2048,128]{1,0:T(8,128)(2,1)} %param.24), kind=kOutput, calls=%fused_computation.22 | convolution fusion | flops 33562624 | bytes 802816 | tf_op jit(solution)/shard_map/dot_general | solution.py:71
  30.0 0.7 copy.66
  30.7 3.5 %all-to-all-start = ((bf16[4,64,128]{2,0,1:T(4,128)(2,1)}), bf16[4,64,128]{2,0,1:T(4,128)(2,1)S(1)}, u32[]{:S(2)}, u32[]{:S(2)}) async-start(bf16[4,64,128]{2,0,1:T(4,128)(2,1)} %copy.66), calls=%async_computation | async-start | bytes 131072 | tf_op jit(solution)/shard_map/all_to_all | solution.py:75
  34.2 0.7 log_bitcast_fusion
  34.9 0.8 convert_reduce_fusion.1
  35.7 5.3 %all-to-all-done = bf16[4,64,128]{2,0,1:T(4,128)(2,1)S(1)} async-done(((bf16[4,64,128]{2,0,1:T(4,128)(2,1)}), bf16[4,64,128]{2,0,1:T(4,128)(2,1)S(1)}, u32[]{:S(2)}, u32[]{:S(2)}) %all-to-all-start) | async-done | bytes 65568 | tf_op jit(solution)/shard_map/all_to_all | solution.py:75
  41.2 4.4 %multiply_add_fusion = f32[4,16,128,128]{3,2,1,0:T(8,128)S(1)} fusion(f32[4,16,128,128]{3,2,1,0:T(8,128)} %param.17, f32[4,16,128]{2,1,0:T(8,128)S(1)} %fusion.57, f32[4,16,128]{2,1,0:T(8,128)S(1)} %get-tuple-element.3, f32[4,16,128]{2,1,0:T(8,128)S(1)} %get-tuple-element.2), kind=kLoop, calls=%fused_computation.6 | loop fusion | flops 3145728 | bytes 8486912 | tf_op jit(solution)/shard_map/add | solution.py:33
  45.6 2.0 %copy-done.1 = f32[4,16,128,128]{3,2,1,0:T(8,128)} copy-done((f32[4,16,128,128]{3,2,1,0:T(8,128)}, f32[4,16,128,128]{3,2,1,0:T(8,128)S(1)}, u32[]{:S(2)}) %copy-start.1) | copy-done | bytes 4194328
  47.6 3.6 %fusion.73 = f32[4,16,1,128]{3,2,1,0:T(1,128)S(1)} fusion(f32[4,16,128,1]{2,3,1,0:T(1,128)S(1)} %bitcast.137, f32[4,16,128,128]{3,2,1,0:T(8,128)S(1)} %multiply_add_fusion), kind=kOutput, calls=%fused_computation.103 | convolution fusion | flops 12582912 | bytes 4259840 | tf_op jit(solution)/shard_map/thk,thkv->thv/dot_general | solution.py:36
  51.3 0.1 multiply_reduce_fusion.2
  51.5 18.4 %all-gather.1 = bf16[16,4,2048]{2,1,0:T(4,128)(2,1)S(1)} all-gather(bf16[1,4,2048]{2,1,0:T(4,128)(2,1)S(1)} %reshape.164), channel_id=1, replica_groups=mesh['grp'=2,'ep'=16] {'ep'}, dimensions={0}, use_global_device_ids=true | all-gather | bytes 278528 | tf_op jit(solution)/shard_map/all_gather | solution.py:78
  70.0 0.8 convolution_convert_fusion.1
  70.8 3.5 %all-to-all-start.1 = ((bf16[16,4,128]{2,1,0:T(4,128)(2,1)}), bf16[16,4,128]{2,1,0:T(4,128)(2,1)S(1)}, u32[]{:S(2)}, u32[]{:S(2)}) async-start(bf16[16,4,128]{2,1,0:T(4,128)(2,1)} %bitcast.21), calls=%async_computation.1 | async-start | bytes 32768 | tf_op jit(solution)/shard_map/all_to_all | solution.py:80
  74.3 6.5 %all-to-all-done.1 = bf16[16,4,128]{2,1,0:T(4,128)(2,1)S(1)} async-done(((bf16[16,4,128]{2,1,0:T(4,128)(2,1)}), bf16[16,4,128]{2,1,0:T(4,128)(2,1)S(1)}, u32[]{:S(2)}, u32[]{:S(2)}) %all-to-all-start.1) | async-done | bytes 16416 | tf_op jit(solution)/shard_map/all_to_all | solution.py:80
  80.8 0.1 multiply_reduce_fusion.1
  80.9 0.2 convolution_convert_fusion
  81.2 0.1 broadcast_in_dim.2
  81.3 12.6 %all_to_all.38 = bf16[16,3,2048]{2,1,0:T(4,128)(2,1)S(1)} all-to-all(bf16[16,3,2048]{2,1,0:T(4,128)(2,1)S(1)} %bitcast.130), channel_id=1, replica_groups=mesh['grp'=2,'ep'=16] {'ep'}, dimensions={0} | all-to-all | bytes 393216 | tf_op jit(solution)/shard_map/all_to_all | solution.py:99
  93.9 4.5 %fusion.4 = f32[16,3,1792]{2,0,1:T(8,128)S(1)} fusion(bf16[2048,1792]{1,0:T(8,128)(2,1)} %param.29, bf16[16,3,2048]{2,1,0:T(4,128)(2,1)S(1)} %all_to_all.38), kind=kOutput, calls=%fused_computation.4 | convolution fusion | flops 352321536 | bytes 7880704 | tf_op jit(solution)/shard_map/scd,df->scf/dot_general | solution.py:100
  98.5 7.9 %fusion.12 = bf16[16,3,2048]{2,0,1:T(8,128)(2,1)S(1)} fusion(bf16[1792,2048]{1,0:T(8,128)(2,1)} %param.31, bf16[2048,1792]{1,0:T(8,128)(2,1)} %param.30, f32[16,3,1792]{2,0,1:T(8,128)S(1)} %fusion.4, bf16[16,3,2048]{2,1,0:T(4,128)(2,1)S(1)} %all_to_all.38), kind=kOutput, calls=%fused_computation.9 | convolution fusion | flops 705257472 | bytes 15417344 | tf_op jit(solution)/shard_map/scf,fd->scd/dot_general | solution.py:103
  106.4 0.9 copy.73
  107.2 3.5 %all-to-all-start.3 = ((bf16[16,3,2048]{2,1,0:T(4,128)(2,1)}), bf16[16,3,2048]{2,1,0:T(4,128)(2,1)S(1)}, u32[]{:S(2)}, u32[]{:S(2)}) async-start(bf16[16,3,2048]{2,1,0:T(4,128)(2,1)} %copy.73), calls=%async_computation.3 | async-start | bytes 524288 | tf_op jit(solution)/shard_map/all_to_all | solution.py:106
  110.8 0.1 fusion.63
  110.9 9.9 %all-to-all-done.3 = bf16[16,3,2048]{2,1,0:T(4,128)(2,1)S(1)} async-done(((bf16[16,3,2048]{2,1,0:T(4,128)(2,1)}), bf16[16,3,2048]{2,1,0:T(4,128)(2,1)S(1)}, u32[]{:S(2)}, u32[]{:S(2)}) %all-to-all-start.3) | async-done | bytes 196640 | tf_op jit(solution)/shard_map/all_to_all | solution.py:106
  120.7 0.1 convert_reduce_fusion
  120.9 0.9 fusion.16
  (31 shorter events, 0.5 us)
Async XLA Ops:
  0.6 25.2 %copy-start = (bf16[2048,128]{1,0:T(8,128)(2,1)S(1)}, bf16[2048,128]{1,0:T(8,128)(2,1)}, u32[]{:S(2)}) copy-start(bf16[2048,128]{1,0:T(8,128)(2,1)} %param.21) | copy-start | bytes 1572868
  28.7 22.7 %copy-start.5 = (f32[128]{0:T(128)S(1)}, f32[128]{0:T(128)}, u32[]{:S(2)}) copy-start(f32[128]{0:T(128)} %param.26) | copy-start | bytes 1540
  30.0 40.0 %copy-start.2 = (bf16[2048,128]{1,0:T(8,128)(2,1)S(1)}, bf16[2048,128]{1,0:T(8,128)(2,1)}, u32[]{:S(2)}) copy-start(bf16[2048,128]{1,0:T(8,128)(2,1)} %param.27) | copy-start | bytes 1572868
  30.7 10.4 %all-to-all-start = ((bf16[4,64,128]{2,0,1:T(4,128)(2,1)}), bf16[4,64,128]{2,0,1:T(4,128)(2,1)S(1)}, u32[]{:S(2)}, u32[]{:S(2)}) async-start(bf16[4,64,128]{2,0,1:T(4,128)(2,1)} %copy.66), calls=%async_computation | async-start | bytes 131072 | tf_op jit(solution)/shard_map/all_to_all | solution.py:75
  41.1 39.7 %copy-start.3 = (bf16[4,2048]{1,0:T(4,128)(2,1)S(1)}, bf16[4,2048]{1,0:T(4,128)(2,1)}, u32[]{:S(2)}) copy-start(bf16[4,2048]{1,0:T(4,128)(2,1)} %param.16) | copy-start | bytes 49156
  41.1 39.8 %copy-start.6 = (f32[2048]{0:T(1024)S(1)}, f32[2048]{0:T(1024)}, u32[]{:S(2)}) copy-start(f32[2048]{0:T(1024)} %param.28) | copy-start | bytes 24580
  45.6 2.0 %copy-start.1 = (f32[4,16,128,128]{3,2,1,0:T(8,128)}, f32[4,16,128,128]{3,2,1,0:T(8,128)S(1)}, u32[]{:S(2)}) copy-start(f32[4,16,128,128]{3,2,1,0:T(8,128)S(1)} %multiply_add_fusion) | copy-start | bytes 12582916
  70.8 10.0 %all-to-all-start.1 = ((bf16[16,4,128]{2,1,0:T(4,128)(2,1)}), bf16[16,4,128]{2,1,0:T(4,128)(2,1)S(1)}, u32[]{:S(2)}, u32[]{:S(2)}) async-start(bf16[16,4,128]{2,1,0:T(4,128)(2,1)} %bitcast.21), calls=%async_computation.1 | async-start | bytes 32768 | tf_op jit(solution)/shard_map/all_to_all | solution.py:80
  98.4 12.3 %copy-start.7 = (bf16[4,2]{0,1:T(2,128)(2,1)S(1)}, bf16[4,2]{0,1:T(2,128)(2,1)}, u32[]{:S(2)}) copy-start(bf16[4,2]{0,1:T(2,128)(2,1)} %param.19) | copy-start | bytes 52
  98.5 12.3 %copy-start.4 = (s32[4,2]{0,1:T(2,128)S(1)}, s32[4,2]{0,1:T(2,128)}, u32[]{:S(2)}) copy-start(s32[4,2]{0,1:T(2,128)} %param.18) | copy-start | bytes 100
  107.2 13.5 %all-to-all-start.3 = ((bf16[16,3,2048]{2,1,0:T(4,128)(2,1)}), bf16[16,3,2048]{2,1,0:T(4,128)(2,1)S(1)}, u32[]{:S(2)}, u32[]{:S(2)}) async-start(bf16[16,3,2048]{2,1,0:T(4,128)(2,1)} %copy.73), calls=%async_computation.3 | async-start | bytes 524288 | tf_op jit(solution)/shard_map/all_to_all | solution.py:106
where the time goes:
time: 123 us; the launch traced here: 122 us
  blocking collectives  55.2 us (45%)
  matrix products  22.1 us (18%)
  waiting for transfers between devices  21.7 us (18%)
  starting transfers between devices  10.5 us (9%)
  other arithmetic  7.51 us (6%)
  local copies, waits for them, and re-layouts  3.88 us (3%)
    all_gather x1, blocking collectives, local(): lax.all_gather(tokens, 'ep', axis=0, tiled=True)  24.2 us
    all_gather x1, blocking collectives, local(): lax.all_gather(mixed, 'ep', axis=0, tiled=True)  18.4 us
    all_to_all x1, blocking collectives, local(): lax.all_to_all(outgoing, 'ep', split_axis=0, concat_axis=0, tiled=True)  12.6 us
    all_to_all x1, waiting for transfers between devices, local(): lax.all_to_all(partial_rows.astype(jnp.bfloat16), 'ep', split_axis=0, con...  9.86 us
    dot_general x1, matrix products, local(): jnp.einsum('scf,fd->scd', hidden, expert_down, preferred_element_type=jnp...  7.88 us
    all_to_all x1, waiting for transfers between devices, local(): lax.all_to_all(mixer_cols, 'ep', split_axis=0, concat_axis=1, tiled=True)  6.45 us
    all_to_all x1, waiting for transfers between devices, local(): lax.all_to_all(projected, 'ep', split_axis=1, concat_axis=2, tiled=True)  5.34 us
    dot_general x1, matrix products, local(): jnp.einsum('scd,df->scf', arrived, expert_gate, preferred_element_type=jn...  4.49 us
  transfers between devices with their start and end apart: 3, of which 3 were waited for; matrix products, arithmetic and copies ran while one was open for 1% of the time, Pallas kernels for 0%

commit v1 on v0

v1 whole, which is shorter than its diff:
```python
import functools

import jax
import jax.numpy as jnp
from jax import lax
from jax.experimental import pallas as pl
from jax.experimental.pallas import tpu as pltpu
from jax.sharding import PartitionSpec as P

FF = 7168
EXPERTS = 4
LANES = 128
MIB = 1 << 20
COST = 10**10

epsilon = 1e-06
f32 = jnp.float32
bf16 = jnp.bfloat16


def call(body, outs, args, name, limit, spaces=None, scratch=(), flops=0, **kwargs):
    spaces = spaces or [pltpu.VMEM] * len(args)
    return pl.pallas_call(
        body,
        out_shape=outs,
        in_specs=[pl.BlockSpec(memory_space=space) for space in spaces],
        out_specs=jax.tree.map(lambda _: pl.BlockSpec(memory_space=pltpu.VMEM), outs),
        scratch_shapes=list(scratch),
        compiler_params=pltpu.CompilerParams(vmem_limit_bytes=limit * MIB),
        cost_estimate=pl.CostEstimate(flops=flops, bytes_accessed=0, transcendentals=0),
        name=name,
        **kwargs,
    )(*args)


def exchange(chunks):
    return lax.all_to_all(chunks, "ep", split_axis=0, concat_axis=0, tiled=True)


def rms(values):
    return values * lax.rsqrt(jnp.mean(values * values, axis=-1, keepdims=True) + epsilon)


def unpack(source, target):
    count, rows = source.shape[0], source.shape[1]
    for i in range(count):
        target[i * rows : (i + 1) * rows, :] = source[i].astype(f32)


def spread_body(rows_ref, out_ref):
    for i in range(out_ref.shape[0]):
        out_ref[i] = rows_ref[...]


def load_body(count, *refs):
    sources, targets, sems = refs[1 : 1 + count], refs[1 + count : 1 + 2 * count], refs[1 + 2 * count]
    copies = [
        pltpu.make_async_copy(source, target, sems.at[i])
        for i, (source, target) in enumerate(zip(sources, targets))
    ]
    for copy in copies:
        copy.start()
    for copy in copies:
        copy.wait()


def load(after, arrays):
    count = len(arrays)
    size = sum(a.size * a.dtype.itemsize for a in arrays)
    return call(
        functools.partial(load_body, count),
        [pltpu.VMEM(a.shape, a.dtype) for a in arrays],
        (after, *arrays),
        "load",
        -(-size // MIB) + 2,
        spaces=[pltpu.VMEM] + [pltpu.HBM] * count,
        scratch=[pltpu.SemaphoreType.DMA((count,))],
        flops=10**9,
    )


def project_body(all_ref, gain_ref, wq_ref, wf_ref, wi_ref, wg_ref, out_ref, rows_ref):
    rows, cols = all_ref.shape[1], wq_ref.shape[1]
    unpack(all_ref, rows_ref)
    normed = (rms(rows_ref[...]) * gain_ref[...]).astype(bf16)
    for p, w_ref in enumerate((wq_ref, wf_ref, wi_ref, wg_ref)):
        product = jnp.dot(normed, w_ref[...], preferred_element_type=f32)
        for i in range(out_ref.shape[0]):
            out_ref[i, :, p * cols : (p + 1) * cols] = product[i * rows : (i + 1) * rows, :].astype(bf16)


def mixer_body(owned_ref, state_ref, bound_ref, gain_ref, out_ref, gates_ref, raw_ref, bounds_ref, read_ref):
    heads, rows = owned_ref.shape[0], owned_ref.shape[1]
    dim = bound_ref.shape[1]
    unpack(owned_ref, raw_ref)
    for h in range(heads):
        bounds_ref[h * rows : (h + 1) * rows, :] = jnp.broadcast_to(bound_ref[h : h + 1, :], (rows, dim))
    bound = bounds_ref[...]
    query_raw, forget_raw, input_raw, gate_raw = (raw_ref[:, p * dim : (p + 1) * dim] for p in range(4))
    decay = bound + (1.0 - bound) * jax.nn.sigmoid(forget_raw)
    key_vec = (1.0 - bound) * jax.nn.sigmoid(-forget_raw)
    query_vec = query_raw * jax.nn.sigmoid(query_raw) * dim ** (-0.5)
    gates_ref[0] = decay
    gates_ref[1] = key_vec
    gates_ref[2] = input_raw
    weights = query_vec * decay
    for start in range(0, heads * rows, 8):
        columns = weights[start : start + 8, :].T
        for p in range(start, min(start + 8, heads * rows)):
            column = columns[:, p - start : p - start + 1]
            read_ref[p : p + 1, :] = jnp.sum(column * state_ref[p % rows, p // rows], axis=0, keepdims=True)
    read = read_ref[...] + jnp.sum(query_vec * key_vec, axis=-1, keepdims=True) * input_raw
    mixed = rms(read) * gain_ref[...] * (gate_raw * jax.nn.sigmoid(gate_raw))
    for h in range(heads):
        block = mixed[h * rows : (h + 1) * rows, :].astype(bf16)
        for i in range(out_ref.shape[0]):
            out_ref[i, :, h * dim : (h + 1) * dim] = block


def update_body(heads_step, gates_ref, state_ref, out_ref, held_ref, in_sem, out_sem):
    rows, heads, dim = state_ref.shape[:3]
    steps = heads // heads_step
    take = rows * heads_step

    def fetch(g):
        part = pl.ds(g * heads_step, heads_step)
        return pltpu.make_async_copy(state_ref.at[:, part], held_ref.at[:, part], in_sem.at[g])

    def put(g):
        part = pl.ds(g * heads_step, heads_step)
        return pltpu.make_async_copy(held_ref.at[:, part], out_ref.at[:, part], out_sem.at[g])

    for g in range(steps):
        fetch(g).start()

    def step(g, carry):
        fetch(g).wait()
        group = pl.ds(g * take, take)
        decay, key_vec = gates_ref[0, group, :].T, gates_ref[1, group, :].T
        value = gates_ref[2, group, :]
        for j in range(take):
            t, h = j % rows, g * heads_step + j // rows
            held_ref[t, h] = decay[:, j : j + 1] * held_ref[t, h] + key_vec[:, j : j + 1] * value[j : j + 1, :]
        put(g).start()
        return carry

    lax.fori_loop(0, steps, step, 0)
    for g in range(steps):
        put(g).wait()


def update(gates, state):
    rows, heads = state.shape[:2]
    heads_step = max(1, 8 // rows)
    steps = heads // heads_step
    return pl.pallas_call(
        functools.partial(update_body, heads_step),
        out_shape=jax.ShapeDtypeStruct(state.shape, f32),
        in_specs=[pl.BlockSpec(memory_space=pltpu.VMEM), pl.BlockSpec(memory_space=pltpu.HBM)],
        out_specs=pl.BlockSpec(memory_space=pltpu.HBM),
        scratch_shapes=[
            pltpu.VMEM(state.shape, f32),
            pltpu.SemaphoreType.DMA((steps,)),
            pltpu.SemaphoreType.DMA((steps,)),
        ],
        compiler_params=pltpu.CompilerParams(vmem_limit_bytes=8 * MIB),
        cost_estimate=pl.CostEstimate(flops=10**9, bytes_accessed=0, transcendentals=0),
        name="update",
    )(gates, state)


def out_body(all_ref, w_ref, out_ref, rows_ref):
    unpack(all_ref, rows_ref)
    product = jnp.dot(rows_ref[...].astype(bf16), w_ref[...], preferred_element_type=f32).astype(bf16)
    for i in range(out_ref.shape[0]):
        out_ref[i] = product


def middle_of(tokens_ref, mixer_ref, target):
    cols = mixer_ref.shape[2]
    unpack(tokens_ref, target)
    for i in range(mixer_ref.shape[0]):
        part = slice(i * cols, (i + 1) * cols)
        target[:, part] = target[:, part] + mixer_ref[i].astype(f32)


def expert_body(tokens_ref, mixer_ref, gain_ref, gate_ref, up_ref, down_ref, out_ref, rows_ref):
    rows = out_ref.shape[1]
    middle_of(tokens_ref, mixer_ref, rows_ref)
    normed = (rms(rows_ref[...]) * gain_ref[...]).astype(bf16)
    gate_act = jnp.dot(normed, gate_ref[...], preferred_element_type=f32)
    up_act = jnp.dot(normed, up_ref[...], preferred_element_type=f32)
    hidden = (gate_act * jax.nn.sigmoid(gate_act) * up_act).astype(bf16)
    product = jnp.dot(hidden, down_ref[...], preferred_element_type=f32)
    for i in range(out_ref.shape[0]):
        out_ref[i] = product[i * rows : (i + 1) * rows, :].astype(bf16)


def own_body(tokens_ref, mixer_ref, out_ref, rows_ref):
    rows = out_ref.shape[0]
    me = lax.axis_index("ep")
    middle_of(tokens_ref, mixer_ref, rows_ref)
    total = jnp.zeros(out_ref.shape, f32)
    for i in range(tokens_ref.shape[0]):
        total = jnp.where(me == i, rows_ref[i * rows : (i + 1) * rows, :], total)
    out_ref[...] = total


def final_body(group, middle_ref, returned_ref, ids_ref, weights_ref, out_ref, shares_ref):
    total = middle_ref[...]
    rows = total.shape[0]
    ids, weights = ids_ref[...], weights_ref[...].astype(f32)
    shares_ref[...] = jnp.zeros(shares_ref.shape, f32)
    for e in range(EXPERTS):
        shares_ref[e : e + 1, :rows] = jnp.sum(jnp.where(ids == e, weights, 0.0), axis=0, keepdims=True)
    shares = shares_ref[...].T
    for e in range(EXPERTS):
        share = shares[:rows, e : e + 1]
        summed = returned_ref[e * group].astype(f32)
        for i in range(e * group + 1, (e + 1) * group):
            summed = summed + returned_ref[i].astype(f32)
        total = total + share * summed
    out_ref[...] = total.astype(bf16)


def local(
    tokens,
    state,
    route_ids,
    route_weights,
    norm_mix,
    w_query,
    w_forget,
    w_input,
    w_gate,
    lower_bound,
    head_gain,
    w_out,
    norm_ffn,
    expert_gate,
    expert_up,
    expert_down,
):
    rows, width = tokens.shape
    heads, dim = state.shape[1], state.shape[2]
    copies = lax.axis_size("ep")
    cols = w_query.shape[1]
    everyone = copies * rows
    group = FF // expert_gate.shape[1]
    shape = jax.ShapeDtypeStruct
    full = shape((copies, rows, width), bf16)

    sent = call(spread_body, full, (tokens,), "spread", 4, flops=COST)
    state_in = state
    all_tokens = exchange(sent)
    projected = call(
        project_body,
        shape((copies, rows, 4 * cols), bf16),
        (all_tokens, norm_mix.reshape(1, width), w_query, w_forget, w_input, w_gate),
        "project",
        8,
        flops=COST,
        scratch=[pltpu.VMEM((everyone, width), f32)],
    )
    owned = exchange(projected)
    if cols != dim:
        owned = owned.reshape(copies, rows, 4, cols).transpose(1, 2, 0, 3).reshape(rows, 4, heads, dim)
        owned = owned.transpose(2, 0, 1, 3).reshape(heads, rows, 4 * dim)
    mixed, gates = call(
        mixer_body,
        [full, shape((3, heads * rows, dim), f32)],
        (owned, state_in, lower_bound.reshape(heads, dim), head_gain.reshape(1, dim)),
        "mixer",
        12,
        flops=COST,
        scratch=[
            pltpu.VMEM((heads * rows, 4 * dim), f32),
            pltpu.VMEM((heads * rows, dim), f32),
            pltpu.VMEM((heads * rows, dim), f32),
        ],
    )
    all_mixed = exchange(mixed)
    mixer_cols = call(
        out_body,
        shape((copies, everyone, cols), bf16),
        (all_mixed, w_out),
        "outward",
        4,
        flops=COST,
        scratch=[pltpu.VMEM((everyone, width), f32)],
    )
    mixer_all = exchange(mixer_cols)
    if cols % LANES:
        mixer_all = mixer_all.transpose(1, 0, 2).reshape(1, everyone, width)
    partials = call(
        expert_body,
        full,
        (all_tokens, mixer_all, norm_ffn.reshape(1, width), expert_gate, expert_up, expert_down),
        "experts",
        30,
        scratch=[pltpu.VMEM((everyone, width), f32)],
    )
    new_state = update(*lax.optimization_barrier((gates, state, partials))[:2])
    returned = exchange(partials)
    middle = call(
        own_body,
        shape((rows, width), f32),
        lax.optimization_barrier((all_tokens, mixer_all, partials))[:2],
        "own",
        4,
        scratch=[pltpu.VMEM((everyone, width), f32)],
        flops=10**8,
    )
    layer_out = call(
        functools.partial(final_body, group),
        shape((rows, width), bf16),
        (middle, returned, route_ids.T, route_weights.T),
        "final",
        4,
        scratch=[pltpu.VMEM((8, LANES), f32)],
    )
    return (layer_out, new_state)


def solution(mesh):
    return jax.shard_map(
        local,
        mesh=mesh,
        in_specs=(
            P(("grp", "ep"), None),
            P(("grp", "ep"), None, None, None),
            P(("grp", "ep"), None),
            P(("grp", "ep"), None),
            P(),
            P(None, "ep"),
            P(None, "ep"),
            P(None, "ep"),
            P(None, "ep"),
            P(),
            P(),
            P(None, "ep"),
            P(),
            P(None, "ep"),
            P(None, "ep"),
            P("ep", None),
        ),
        out_specs=(P(("grp", "ep"), None), P(("grp", "ep"), None, None, None)),
        check_vma=False,
    )
```

time: 123 us -> 77.2 us (0.63)
  matrix products: 22.1 us -> 0 us
  waiting for transfers between devices: 21.7 us -> 2.23 us
  Pallas kernels: 0 us -> 13.8 us
  other arithmetic: 7.51 us -> 0.01 us
  starting transfers between devices: 10.5 us -> 3.66 us
  blocking collectives: 55.2 us -> 53.1 us
    all_gather x2 -> x0, blocking collectives: 42.6 us -> none  [the longest x1 24.2 us: local(): lax.all_gather(tokens, 'ep', axis=0, tiled=True)]
    all_to_all x1 -> x4, blocking collectives: 12.6 us -> 53.1 us  [exchange(): return lax.all_to_all(chunks, 'ep', split_axis=0, concat_axis=0, tiled=True)]
    dot_general x10 -> x0, matrix products: 22.1 us -> none  [the longest x1 7.88 us: local(): jnp.einsum('scf,fd->scd', hidden, expert_down, preferred_element_type=jnp...]
    all_to_all x3 -> x1, waiting for transfers between devices: 21.7 us -> 2.23 us  [exchange(): return lax.all_to_all(chunks, 'ep', split_axis=0, concat_axis=0, tiled=True)]
    pallas_call x0 -> x8, Pallas kernels: none -> 13.8 us  [the longest x7 8.42 us: call(): pl.pallas_call(body, out_shape=outs, in_specs=[pl.BlockSpec(memory_space=...]
    all_to_all x3 -> x1, starting transfers between devices: 10.5 us -> 3.66 us  [exchange(): return lax.all_to_all(chunks, 'ep', split_axis=0, concat_axis=0, tiled=True)]
    add x1 -> x0, other arithmetic: 4.39 us -> none  [mixer_state(): jnp.exp(log_forget).reshape(head_shape)[..., None] * state]
    reduce_sum x6 -> x0, other arithmetic: 1.33 us -> none  [the longest x1 0.76 us: local(): hit_mask = jnp.sum(matches, axis=1)]
  transfers between devices with their start and end apart: 3 -> 1, of which waited for: 3 -> 1; matrix products, arithmetic and copies ran while one was open for 1% -> 0% of each run, Pallas kernels for 0% -> 7%
where the time goes in v1:
time: 77.2 us; the launch traced here: 76.8 us
  blocking collectives  53.1 us (69%)
  Pallas kernels  13.8 us (18%)
  starting transfers between devices  3.66 us (5%)
  local copies, waits for them, and re-layouts  3.13 us (4%)
  waiting for transfers between devices  2.23 us (3%)
  between operations  0.89 us (1%)
    all_to_all x4, blocking collectives, exchange(): return lax.all_to_all(chunks, 'ep', split_axis=0, concat_axis=0, tiled=True)  53.1 us
    pallas_call x7, Pallas kernels, call(): pl.pallas_call(body, out_shape=outs, in_specs=[pl.BlockSpec(memory_space=...  8.42 us
    pallas_call x1, Pallas kernels, update(): pl.pallas_call(functools.partial(update_body, heads_step), out_shape=jax....  5.36 us
    all_to_all x1, starting transfers between devices, exchange(): return lax.all_to_all(chunks, 'ep', split_axis=0, concat_axis=0, tiled=True)  3.66 us
    unnamed x40, local copies, waits for them, and re-layouts  3.13 us
    all_to_all x1, waiting for transfers between devices, exchange(): return lax.all_to_all(chunks, 'ep', split_axis=0, concat_axis=0, tiled=True)  2.23 us
  transfers between devices with their start and end apart: 1, of which 1 were waited for; matrix products, arithmetic and copies ran while one was open for 0% of the time, Pallas kernels for 7%

profile of v1, /device:TPU:0, one launch (start us, length us, event | category | flops | bytes accessed | tf_op | source)
XLA Modules:
  0.0 76.8 jit_solution(8355712280747291351)
XLA Ops:
  0.6 0.0 copy-start.8
  0.7 0.9 %copy-done.10 = bf16[4,2048]{1,0:T(4,128)(2,1)S(1)} copy-done((bf16[4,2048]{1,0:T(4,128)(2,1)S(1)}, bf16[4,2048]{1,0:T(4,128)(2,1)}, u32[]{:S(2)}) %copy-start.10) | copy-done | bytes 16408
  1.6 17.2 %all_to_all.25.all_ref.tokens_ref = bf16[16,4,2048]{2,1,0:T(4,128)(2,1)S(1)} all-to-all(bf16[16,4,2048]{2,1,0:T(4,128)(2,1)S(1)} %spread.1), channel_id=1, replica_groups=mesh['grp'=2,'ep'=16] {'ep'}, dimensions={0} | all-to-all | bytes 524288 | tf_op jit(solution)/shard_map/all_to_all | solution.py:37
  18.8 0.0 copy-done.7
  18.8 0.0 copy-start
  18.8 0.0 copy-start.12
  18.8 0.0 copy-start.13
  18.9 0.6 project.1
  19.5 9.7 %all_to_all.26.owned_ref = bf16[16,4,512]{2,1,0:T(4,128)(2,1)S(1)} all-to-all(bf16[16,4,512]{2,1,0:T(4,128)(2,1)S(1)} %project.1), channel_id=1, replica_groups=mesh['grp'=2,'ep'=16] {'ep'}, dimensions={0} | all-to-all | bytes 131072 | tf_op jit(solution)/shard_map/all_to_all | solution.py:37
  29.2 0.0 copy-done
  29.2 0.0 copy-start.9
  29.2 0.0 slice-start
  29.2 0.0 slice-start.2
  29.2 0.0 slice-start.4
  29.2 1.7 %mixer.1 = (bf16[16,4,2048]{2,1,0:T(4,128)(2,1)S(1)}, f32[3,64,128]{2,1,0:T(8,128)S(1)}) custom-call(bf16[16,4,512]{2,1,0:T(4,128)(2,1)S(1)} %all_to_all.26.owned_ref, f32[4,16,128,128]{3,2,1,0:T(8,128)S(1)} %copy-done, f32[16,128]{1,0:T(8,128)S(1)} %bitcast.16, f32[1,128]{1,0:T(1,128)S(1)} %bitcast.17), custom_call_target="tpu_custom_call" | custom-call | flops 10000000000 | tf_op jit(solution)/shard_map/mixer/pallas_call | solution.py:23
  30.9 13.0 %all_to_all.27.all_ref = bf16[16,4,2048]{2,1,0:T(4,128)(2,1)S(1)} all-to-all(bf16[16,4,2048]{2,1,0:T(4,128)(2,1)S(1)} %get-tuple-element.8), channel_id=1, replica_groups=mesh['grp'=2,'ep'=16] {'ep'}, dimensions={0} | all-to-all | bytes 524288 | tf_op jit(solution)/shard_map/all_to_all | solution.py:37
  43.9 0.0 copy-start.2
  43.9 0.3 outward.1
  44.2 13.1 %all_to_all.28.mixer_ref = bf16[16,64,128]{2,1,0:T(8,128)(2,1)S(1)} all-to-all(bf16[16,64,128]{2,1,0:T(8,128)(2,1)S(1)} %outward.1), channel_id=1, replica_groups=mesh['grp'=2,'ep'=16] {'ep'}, dimensions={0} | all-to-all | bytes 524288 | tf_op jit(solution)/shard_map/all_to_all | solution.py:37
  57.3 0.0 slice-done.4
  57.4 0.0 slice-done.1
  57.4 0.0 slice-done.3
  57.4 0.0 slice-done.5
  57.4 0.0 copy-done.2
  57.4 4.9 %experts.1 = bf16[16,4,2048]{2,1,0:T(4,128)(2,1)} custom-call(bf16[16,4,2048]{2,1,0:T(4,128)(2,1)S(1)} %all_to_all.25.all_ref.tokens_ref, bf16[16,64,128]{2,1,0:T(8,128)(2,1)S(1)} %all_to_all.28.mixer_ref, f32[1,2048]{1,0:T(1,128)S(1)} %bitcast.12, bf16[2048,1792]{1,0:T(8,128)(2,1)S(1)} %bitcast.7, bf16[2048,1792]{1,0:T(8,128)(2,1)S(1)} %bitcast.9, ...), custom_call_target="tpu_custom_call" | custom-call | tf_op jit(solution)/shard_map/experts/pallas_call | solution.py:23
  62.3 3.7 %all-to-all-start.4 = ((bf16[16,4,2048]{2,1,0:T(4,128)(2,1)}), bf16[16,4,2048]{2,1,0:T(4,128)(2,1)S(1)}, u32[]{:S(2)}, u32[]{:S(2)}) async-start(bf16[16,4,2048]{2,1,0:T(4,128)(2,1)} %experts.1), calls=%async_computation.4 | async-start | bytes 524288 | tf_op jit(solution)/shard_map/all_to_all | solution.py:37
  66.0 0.2 own.1.middle_ref
  66.2 0.0 copy-start.1
  66.2 2.2 %copy-done.1 = f32[4,16,128,128]{3,2,1,0:T(8,128)S(1)} copy-done((f32[4,16,128,128]{3,2,1,0:T(8,128)S(1)}, f32[4,16,128,128]{3,2,1,0:T(8,128)}, u32[]{:S(2)}) %copy-start.1) | copy-done | bytes 4194328
  68.4 5.4 %update.1 = f32[4,16,128,128]{3,2,1,0:T(8,128)} custom-call(f32[3,64,128]{2,1,0:T(8,128)S(1)} %get-tuple-element.12.gates_ref, f32[4,16,128,128]{3,2,1,0:T(8,128)S(1)} %copy-done.1), custom_call_target="tpu_custom_call" | custom-call | flops 1000000000 | tf_op jit(solution)/shard_map/update/pallas_call | solution.py:156
  73.8 2.2 %all-to-all-done.4.returned_ref = bf16[16,4,2048]{2,1,0:T(4,128)(2,1)S(1)} async-done(((bf16[16,4,2048]{2,1,0:T(4,128)(2,1)}), bf16[16,4,2048]{2,1,0:T(4,128)(2,1)S(1)}, u32[]{:S(2)}, u32[]{:S(2)}) %all-to-all-start.4) | async-done | bytes 262176 | tf_op jit(solution)/shard_map/all_to_all | solution.py:37
  76.0 0.8 %final.1 = bf16[4,2048]{1,0:T(4,128)(2,1)} custom-call(f32[4,2048]{1,0:T(4,128)S(1)} %own.1.middle_ref, bf16[16,4,2048]{2,1,0:T(4,128)(2,1)S(1)} %all-to-all-done.4.returned_ref, s32[2,4]{1,0:T(2,128)S(1)} %bitcast.13, bf16[2,4]{1,0:T(2,128)(2,1)S(1)} %bitcast.14), custom_call_target="tpu_custom_call" | custom-call | tf_op jit(solution)/shard_map/final/pallas_call | solution.py:23
  (25 shorter events, 0.1 us)
Async XLA Ops:
  0.6 18.2 %copy-start.8 = (bf16[2048,128]{1,0:T(8,128)(2,1)S(1)}, bf16[2048,128]{1,0:T(8,128)(2,1)}, u32[]{:S(2)}) copy-start(bf16[2048,128]{1,0:T(8,128)(2,1)} %wg_ref.1) | copy-start | bytes 1572868
  0.6 18.1 %copy-start.7 = (bf16[2048,128]{1,0:T(8,128)(2,1)S(1)}, bf16[2048,128]{1,0:T(8,128)(2,1)}, u32[]{:S(2)}) copy-start(bf16[2048,128]{1,0:T(8,128)(2,1)} %wi_ref.1) | copy-start | bytes 1572868
  0.7 18.1 %copy-start.6 = (bf16[2048,128]{1,0:T(8,128)(2,1)S(1)}, bf16[2048,128]{1,0:T(8,128)(2,1)}, u32[]{:S(2)}) copy-start(bf16[2048,128]{1,0:T(8,128)(2,1)} %wf_ref.1) | copy-start | bytes 1572868
  0.7 18.1 %copy-start.5 = (bf16[2048,128]{1,0:T(8,128)(2,1)S(1)}, bf16[2048,128]{1,0:T(8,128)(2,1)}, u32[]{:S(2)}) copy-start(bf16[2048,128]{1,0:T(8,128)(2,1)} %wq_ref.1) | copy-start | bytes 1572868
  0.7 0.9 %copy-start.10 = (bf16[4,2048]{1,0:T(4,128)(2,1)S(1)}, bf16[4,2048]{1,0:T(4,128)(2,1)}, u32[]{:S(2)}) copy-start(bf16[4,2048]{1,0:T(4,128)(2,1)} %rows_ref.1) | copy-start | bytes 49156
  1.5 17.3 %copy-start.11 = (f32[2048]{0:T(1024)S(1)}, f32[2048]{0:T(1024)}, u32[]{:S(2)}) copy-start(f32[2048]{0:T(1024)} %param.20) | copy-start | bytes 24580
  18.8 10.4 %copy-start = (f32[4,16,128,128]{3,2,1,0:T(8,128)S(1)}, f32[4,16,128,128]{3,2,1,0:T(8,128)}, u32[]{:S(2)}) copy-start(f32[4,16,128,128]{3,2,1,0:T(8,128)} %state_ref.2) | copy-start | bytes 12582916
  18.8 10.4 %copy-start.12 = (f32[2048]{0:T(1024)S(1)}, f32[2048]{0:T(1024)}, u32[]{:S(2)}) copy-start(f32[2048]{0:T(1024)} %param.25) | copy-start | bytes 24580
  18.8 10.3 %copy-start.13 = (f32[128]{0:T(128)S(1)}, f32[128]{0:T(128)}, u32[]{:S(2)}) copy-start(f32[128]{0:T(128)} %param.26) | copy-start | bytes 1540
  29.2 14.7 %copy-start.9 = (bf16[2048,128]{1,0:T(8,128)(2,1)S(1)}, bf16[2048,128]{1,0:T(8,128)(2,1)}, u32[]{:S(2)}) copy-start(bf16[2048,128]{1,0:T(8,128)(2,1)} %w_ref.1) | copy-start | bytes 1572868
  29.2 28.1 %slice-start = ((s8[7340032]{0:T(1024)(128)(4,1)}), s8[4194304]{0:T(1024)(128)(4,1)S(1)}, s32[]{:S(2)}) async-start(s8[7340032]{0:T(1024)(128)(4,1)} %bitcast.6), calls=%async_computation.5 | async-start | bytes 8388608
  29.2 28.1 %slice-start.2 = ((s8[7340032]{0:T(1024)(128)(4,1)}), s8[4194304]{0:T(1024)(128)(4,1)S(1)}, s32[]{:S(2)}) async-start(s8[7340032]{0:T(1024)(128)(4,1)} %bitcast.8), calls=%async_computation.7 | async-start | bytes 8388608
  29.2 28.1 %slice-start.4 = ((s8[7340032]{0:T(1024)(128)(4,1)}), s8[4194304]{0:T(1024)(128)(4,1)S(1)}, s32[]{:S(2)}) async-start(s8[7340032]{0:T(1024)(128)(4,1)} %bitcast.10), calls=%async_computation.9 | async-start | bytes 8388608
  43.9 13.4 %slice-start.1 = ((s8[7340032]{0:T(1024)(128)(4,1)}), s8[3145728]{0:T(1024)(128)(4,1)S(1)}, s32[]{:S(2)}) async-start(s8[7340032]{0:T(1024)(128)(4,1)} %bitcast.6), calls=%async_computation.6 | async-start | bytes 6291456
  43.9 13.4 %slice-start.3 = ((s8[7340032]{0:T(1024)(128)(4,1)}), s8[3145728]{0:T(1024)(128)(4,1)S(1)}, s32[]{:S(2)}) async-start(s8[7340032]{0:T(1024)(128)(4,1)} %bitcast.8), calls=%async_computation.8 | async-start | bytes 6291456
  43.9 13.5 %slice-start.5 = ((s8[7340032]{0:T(1024)(128)(4,1)}), s8[3145728]{0:T(1024)(128)(4,1)S(1)}, s32[]{:S(2)}) async-start(s8[7340032]{0:T(1024)(128)(4,1)} %bitcast.10), calls=%async_computation.10 | async-start | bytes 6291456
  43.9 13.5 %copy-start.2 = (f32[2048]{0:T(1024)S(1)}, f32[2048]{0:T(1024)}, u32[]{:S(2)}) copy-start(f32[2048]{0:T(1024)} %param.28) | copy-start | bytes 24580
  62.3 13.7 %copy-start.3 = (s32[4,2]{0,1:T(2,128)S(1)}, s32[4,2]{0,1:T(2,128)}, u32[]{:S(2)}) copy-start(s32[4,2]{0,1:T(2,128)} %param.18) | copy-start | bytes 100
  62.3 13.7 %copy-start.4 = (bf16[4,2]{0,1:T(2,128)(2,1)S(1)}, bf16[4,2]{0,1:T(2,128)(2,1)}, u32[]{:S(2)}) copy-start(bf16[4,2]{0,1:T(2,128)(2,1)} %param.19) | copy-start | bytes 52
  62.3 13.6 %all-to-all-start.4 = ((bf16[16,4,2048]{2,1,0:T(4,128)(2,1)}), bf16[16,4,2048]{2,1,0:T(4,128)(2,1)S(1)}, u32[]{:S(2)}, u32[]{:S(2)}) async-start(bf16[16,4,2048]{2,1,0:T(4,128)(2,1)} %experts.1), calls=%async_computation.4 | async-start | bytes 524288 | tf_op jit(solution)/shard_map/all_to_all | solution.py:37
  66.2 2.2 %copy-start.1 = (f32[4,16,128,128]{3,2,1,0:T(8,128)S(1)}, f32[4,16,128,128]{3,2,1,0:T(8,128)}, u32[]{:S(2)}) copy-start(f32[4,16,128,128]{3,2,1,0:T(8,128)} %state_ref.2) | copy-start | bytes 12582916

commit v2 on v1

v2 whole, which is shorter than its diff:
```python
import functools

import jax
import jax.numpy as jnp
from jax import lax
from jax.experimental import pallas as pl
from jax.experimental.pallas import tpu as pltpu
from jax.sharding import Mesh
from jax.sharding import PartitionSpec as P

FF = 7168
EXPERTS = 4
LANES = 128
MIB = 1 << 20
COST = 10**10

epsilon = 1e-06
f32 = jnp.float32
bf16 = jnp.bfloat16


def call(body, outs, args, limit, spaces=None, scratch=(), flops=0, **kwargs):
    spaces = spaces or [pltpu.VMEM] * len(args)
    return pl.pallas_call(
        body,
        out_shape=outs,
        in_specs=[pl.BlockSpec(memory_space=space) for space in spaces],
        out_specs=jax.tree.map(lambda _: pl.BlockSpec(memory_space=pltpu.VMEM), outs),
        scratch_shapes=list(scratch),
        compiler_params=pltpu.CompilerParams(vmem_limit_bytes=limit * MIB),
        cost_estimate=pl.CostEstimate(flops=flops, bytes_accessed=0, transcendentals=0),
        **kwargs,
    )(*args)


AXES = ("chip", "core")


def exchange(chunks):
    return lax.all_to_all(chunks, "chip", split_axis=0, concat_axis=0, tiled=True)


def swap(values):
    return lax.ppermute(values, "core", [(0, 1), (1, 0)])


def rms(values):
    return values * lax.rsqrt(jnp.mean(values * values, axis=-1, keepdims=True) + epsilon)


def unpack(source, target):
    count, rows = source.shape[0], source.shape[1]
    for i in range(count):
        target[i * rows : (i + 1) * rows, :] = source[i].astype(f32)


def spread_body(rows_ref, out_ref):
    for i in range(out_ref.shape[0]):
        out_ref[i] = rows_ref[...]


def project_body(all_ref, gain_ref, *refs):
    weights, (out_ref, rows_ref) = refs[:8], refs[8:]
    rows, cols = all_ref.shape[1], weights[0].shape[1]
    core = lax.axis_index("core")
    unpack(all_ref, rows_ref)
    normed = (rms(rows_ref[...]) * gain_ref[...]).astype(bf16)
    for i, w_ref in enumerate(weights):
        p, cross = divmod(i, 2)
        side = 1 - core if cross else core
        product = jnp.dot(normed, w_ref[...], preferred_element_type=f32)
        for chip in range(all_ref.shape[0]):
            block = product[chip * rows : (chip + 1) * rows, :].astype(bf16)
            out_ref[chip, side, :, p * cols : (p + 1) * cols] = block


def mixer_body(owned_ref, state_ref, bound_ref, gain_ref, out_ref, gates_ref, raw_ref, bounds_ref, read_ref):
    heads, rows = owned_ref.shape[0], owned_ref.shape[1]
    dim = bound_ref.shape[1]
    for h in range(heads):
        raw_ref[h * rows : (h + 1) * rows, :] = owned_ref[h].astype(f32)
        bounds_ref[h * rows : (h + 1) * rows, :] = jnp.broadcast_to(bound_ref[h : h + 1, :], (rows, dim))
    bound = bounds_ref[...]
    query_raw, forget_raw, input_raw, gate_raw = (raw_ref[:, p * dim : (p + 1) * dim] for p in range(4))
    decay = bound + (1.0 - bound) * jax.nn.sigmoid(forget_raw)
    key_vec = (1.0 - bound) * jax.nn.sigmoid(-forget_raw)
    query_vec = query_raw * jax.nn.sigmoid(query_raw) * dim ** (-0.5)
    gates_ref[0] = decay
    gates_ref[1] = key_vec
    gates_ref[2] = input_raw
    weights = query_vec * decay
    for start in range(0, heads * rows, 8):
        columns = weights[start : start + 8, :].T
        for p in range(start, min(start + 8, heads * rows)):
            column = columns[:, p - start : p - start + 1]
            read_ref[p : p + 1, :] = jnp.sum(column * state_ref[p % rows, p // rows], axis=0, keepdims=True)
    read = read_ref[...] + jnp.sum(query_vec * key_vec, axis=-1, keepdims=True) * input_raw
    mixed = rms(read) * gain_ref[...] * (gate_raw * jax.nn.sigmoid(gate_raw))
    for h in range(heads):
        block = mixed[h * rows : (h + 1) * rows, :].astype(bf16)
        for i in range(out_ref.shape[0]):
            out_ref[i, :, h * dim : (h + 1) * dim] = block


def out_body(all_ref, own_ref, cross_ref, out_ref, rows_ref):
    core = lax.axis_index("core")
    unpack(all_ref, rows_ref)
    mixed = rows_ref[...].astype(bf16)
    for side, w_ref in ((core, own_ref), (1 - core, cross_ref)):
        block = jnp.dot(mixed, w_ref[...], preferred_element_type=f32).astype(bf16)
        for i in range(out_ref.shape[0]):
            out_ref[i, side] = block


def norm_body(tokens_ref, mixer_ref, gain_ref, normed_ref, middle_ref, rows_ref):
    rows, cols = middle_ref.shape[1], mixer_ref.shape[3]
    unpack(tokens_ref, rows_ref)
    for chip in range(mixer_ref.shape[0]):
        for side in range(2):
            part = slice((2 * chip + side) * cols, (2 * chip + side + 1) * cols)
            rows_ref[:, part] = rows_ref[:, part] + mixer_ref[chip, side].astype(f32)
    normed_ref[...] = (rms(rows_ref[...]) * gain_ref[...]).astype(bf16)
    for chip in range(middle_ref.shape[0]):
        middle_ref[chip] = rows_ref[chip * rows : (chip + 1) * rows, :]


def expert_body(
    mine_ref,
    other_ref,
    gate_ref,
    up_ref,
    down_ref,
    gates_ref,
    state_ref,
    keep_ref,
    send_ref,
    new_ref,
    normed_ref,
    hidden_ref,
    held_ref,
    sems,
):
    chips, rows = keep_ref.shape[:2]
    half = mine_ref.shape[0]
    hidden_cols, width = gate_ref.shape[1], down_ref.shape[1]
    seqs, heads = state_ref.shape[:2]
    step = 2 * LANES
    blocks = [pl.ds(i, min(step, hidden_cols - i)) for i in range(0, hidden_cols, step)]
    parts = [pl.ds(i, min(step, width - i)) for i in range(0, width, step)]
    normed_ref[:half, :] = mine_ref[...]
    normed_ref[half:, :] = other_ref[...]
    normed = normed_ref[...]
    copies = []

    def renew(h):
        group = slice(h * seqs, (h + 1) * seqs)
        decay, key_vec, value = gates_ref[0, group, :].T, gates_ref[1, group, :].T, gates_ref[2, group, :]
        for t in range(seqs):
            held_ref[t, h] = decay[:, t : t + 1] * state_ref[t, h] + key_vec[:, t : t + 1] * value[t : t + 1, :]
        copies.append(pltpu.make_async_copy(held_ref.at[:, h], new_ref.at[:, h], sems.at[h]))
        copies[-1].start()

    for i, block in enumerate(blocks):
        gate_act = jnp.dot(normed, gate_ref[:, block], preferred_element_type=f32)
        up_act = jnp.dot(normed, up_ref[:, block], preferred_element_type=f32)
        for h in range(i * heads // len(blocks), (i + 1) * heads // len(blocks)):
            renew(h)
        hidden_ref[:, block] = (gate_act * jax.nn.sigmoid(gate_act) * up_act).astype(bf16)
    hidden = hidden_ref[...]
    for part in parts:
        product = jnp.dot(hidden, down_ref[:, part], preferred_element_type=f32)
        for side, out_ref in enumerate((keep_ref, send_ref)):
            for chip in range(chips):
                start = (side * chips + chip) * rows
                out_ref[chip, :, part] = product[start : start + rows, :].astype(out_ref.dtype)
    for copy in copies:
        copy.wait()


def add_body(keep_ref, came_ref, out_ref):
    out_ref[...] = (keep_ref[...] + came_ref[...].astype(f32)).astype(bf16)


def final_body(group, middle_ref, returned_ref, ids_ref, weights_ref, out_ref, shares_ref):
    total = middle_ref[lax.axis_index("chip")]
    rows = total.shape[0]
    ids, weights = ids_ref[...], weights_ref[...].astype(f32)
    shares_ref[...] = jnp.zeros(shares_ref.shape, f32)
    for e in range(EXPERTS):
        shares_ref[e : e + 1, :rows] = jnp.sum(jnp.where(ids == e, weights, 0.0), axis=0, keepdims=True)
    shares = shares_ref[...].T
    for e in range(EXPERTS):
        share = shares[:rows, e : e + 1]
        summed = returned_ref[e * group].astype(f32)
        for i in range(e * group + 1, (e + 1) * group):
            summed = summed + returned_ref[i].astype(f32)
        total = total + share * summed
    out_ref[...] = total.astype(bf16)


def body(
    tokens,
    state,
    route_ids,
    route_weights,
    norm_mix,
    w_query,
    w_forget,
    w_input,
    w_gate,
    lower_bound,
    head_gain,
    w_out,
    norm_ffn,
    expert_gate,
    expert_up,
    expert_down,
):
    rows, width = tokens.shape
    heads, dim = state.shape[1], state.shape[2]
    chips = lax.axis_size("chip")
    cols = w_query.shape[1]
    half = chips * rows
    group = FF // expert_gate.shape[1] // 2
    shape = jax.ShapeDtypeStruct
    full = shape((chips, rows, width), bf16)
    rows_scratch = [pltpu.VMEM((half, width), f32)]

    weights = []
    for weight in (w_query, w_forget, w_input, w_gate, w_out):
        weights += [weight, swap(weight)]
    sent = call(spread_body, full, (tokens,), 4, flops=COST)
    all_tokens = exchange(sent)
    all_tokens, out_cross = lax.optimization_barrier((all_tokens, weights[9]))
    projected = call(
        project_body,
        shape((chips, 2, rows, 4 * cols), bf16),
        (all_tokens, norm_mix.reshape(1, width), *weights[:8]),
        8,
        scratch=rows_scratch,
        flops=COST,
    )
    owned = exchange(projected).reshape(2 * chips, rows, 4 * cols)
    if cols != dim:
        owned = owned.reshape(2 * chips, rows, 4, cols).transpose(1, 2, 0, 3).reshape(rows, 4, heads, dim)
        owned = owned.transpose(2, 0, 1, 3).reshape(heads, rows, 4 * dim)
    mixed, gates = call(
        mixer_body,
        [full, shape((3, heads * rows, dim), f32)],
        (owned, state, lower_bound.reshape(heads, dim), head_gain.reshape(1, dim)),
        12,
        flops=COST,
        scratch=[
            pltpu.VMEM((heads * rows, 4 * dim), f32),
            pltpu.VMEM((heads * rows, dim), f32),
            pltpu.VMEM((heads * rows, dim), f32),
        ],
    )
    mixer_cols = call(
        out_body,
        shape((chips, 2, half, cols), bf16),
        (exchange(mixed), w_out, out_cross),
        6,
        flops=COST,
        scratch=rows_scratch,
    )
    normed, middle = call(
        norm_body,
        [shape((half, width), bf16), shape((chips, rows, width), f32)],
        (all_tokens, exchange(mixer_cols), norm_ffn.reshape(1, width)),
        6,
        flops=COST,
        scratch=rows_scratch,
    )
    vmem = pl.BlockSpec(memory_space=pltpu.VMEM)
    keep, send, new_state = pl.pallas_call(
        expert_body,
        out_shape=[shape((chips, rows, width), f32), full, shape(state.shape, f32)],
        in_specs=[vmem] * 7,
        out_specs=[vmem, vmem, pl.BlockSpec(memory_space=pltpu.HBM)],
        scratch_shapes=[
            pltpu.VMEM((2 * half, width), bf16),
            pltpu.VMEM((2 * half, expert_gate.shape[1]), bf16),
            pltpu.VMEM(state.shape, f32),
            pltpu.SemaphoreType.DMA((heads,)),
        ],
        compiler_params=pltpu.CompilerParams(vmem_limit_bytes=14 * MIB),
        cost_estimate=pl.CostEstimate(flops=COST, bytes_accessed=0, transcendentals=0),
        name="experts",
    )(normed, swap(normed), expert_gate, expert_up, expert_down, gates, state)
    partials = call(add_body, full, (keep, swap(send)), 4)
    returned = exchange(partials)
    layer_out = call(
        functools.partial(final_body, group),
        shape((rows, width), bf16),
        (middle, returned, route_ids.T, route_weights.T),
        4,
        scratch=[pltpu.VMEM((8, LANES), f32)],
    )
    return (layer_out, new_state)


def solution(mesh):
    groups, size = mesh.shape["grp"], mesh.shape["ep"]
    split = Mesh(mesh.devices.reshape(groups, size // 2, 2), ("grp", *AXES))
    return jax.shard_map(
        body,
        mesh=split,
        in_specs=(
            P(("grp", *AXES), None),
            P(("grp", *AXES), None, None, None),
            P(("grp", *AXES), None),
            P(("grp", *AXES), None),
            P(),
            P(None, AXES),
            P(None, AXES),
            P(None, AXES),
            P(None, AXES),
            P(),
            P(),
            P(None, AXES),
            P(),
            P(None, AXES),
            P(None, AXES),
            P(AXES, None),
        ),
        out_specs=(P(("grp", *AXES), None), P(("grp", *AXES), None, None, None)),
        check_vma=False,
    )
```

time: 77.2 us -> 69.4 us (0.90)
  Pallas kernels: 13.8 us -> 9.09 us
  local copies, waits for them, and re-layouts: 3.13 us -> 0.82 us
  starting transfers between devices: 3.66 us -> 1.86 us
    pallas_call x7, Pallas kernels: 8.42 us -> 3.79 us  [call(): pl.pallas_call(body, out_shape=outs, in_specs=[pl.BlockSpec(memory_space=...]
    all_to_all x1 -> x0, starting transfers between devices: 3.66 us -> none  [exchange(): return lax.all_to_all(chunks, 'ep', split_axis=0, concat_axis=0, tiled=True)]
    ppermute x0 -> x7, waiting for transfers between devices: none -> 2.55 us  [swap(): return lax.ppermute(values, 'core', [(0, 1), (1, 0)])]
    unnamed x40 -> x38, local copies, waits for them, and re-layouts: 3.13 us -> 0.82 us
    all_to_all x1 -> x0, waiting for transfers between devices: 2.23 us -> none  [exchange(): return lax.all_to_all(chunks, 'ep', split_axis=0, concat_axis=0, tiled=True)]
    ppermute x0 -> x7, starting transfers between devices: none -> 1.86 us  [swap(): return lax.ppermute(values, 'core', [(0, 1), (1, 0)])]
    all_to_all x4 -> x5, blocking collectives: 53.1 us -> 53.8 us  [exchange(): lax.all_to_all(chunks, 'chip', split_axis=0, concat_axis=0, tiled=True)]
  transfers between devices with their start and end apart: 1 -> 7, of which waited for: 1 -> 2; matrix products, arithmetic and copies ran while one was open for 0% -> 0% of each run, Pallas kernels for 7% -> 0%
where the time goes in v2:
time: 69.4 us; the launch traced here: 69 us
  blocking collectives  53.8 us (78%)
  Pallas kernels  9.09 us (13%)
  waiting for transfers between devices  2.55 us (4%)
  starting transfers between devices  1.86 us (3%)
  between operations  0.93 us (1%)
  local copies, waits for them, and re-layouts  0.82 us (1%)
    all_to_all x5, blocking collectives, exchange(): lax.all_to_all(chunks, 'chip', split_axis=0, concat_axis=0, tiled=True)  53.8 us
    pallas_call x1, Pallas kernels, body(): pl.pallas_call(expert_body, out_shape=[shape((chips, rows, width), f32),...  5.3 us
    pallas_call x7, Pallas kernels, call(): pl.pallas_call(body, out_shape=outs, in_specs=[pl.BlockSpec(memory_space=...  3.79 us
    ppermute x7, waiting for transfers between devices, swap(): return lax.ppermute(values, 'core', [(0, 1), (1, 0)])  2.55 us
    ppermute x7, starting transfers between devices, swap(): return lax.ppermute(values, 'core', [(0, 1), (1, 0)])  1.86 us
  transfers between devices with their start and end apart: 7, of which 2 were waited for; matrix products, arithmetic and copies ran while one was open for 0% of the time, Pallas kernels for 0%

profile of v2, /device:TPU:0, one launch (start us, length us, event | category | flops | bytes accessed | tf_op | source)
XLA Modules:
  0.0 69.0 jit_solution(18028191270724613003)
XLA Ops:
  0.7 0.6 collective-permute-start.1
  1.2 0.1 collective-permute-start.2
  1.3 0.4 collective-permute-start.3
  1.7 0.1 collective-permute-start.4
  1.8 0.4 collective-permute-start
  2.3 0.7 %copy-done.8 = bf16[4,2048]{1,0:T(4,128)(2,1)S(1)} copy-done((bf16[4,2048]{1,0:T(4,128)(2,1)S(1)}, bf16[4,2048]{1,0:T(4,128)(2,1)}, u32[]{:S(2)}) %copy-start.8) | copy-done | bytes 16408
  3.0 14.3 %all_to_all.25.all_ref.tokens_ref = bf16[8,4,2048]{2,1,0:T(4,128)(2,1)S(1)} all-to-all(bf16[8,4,2048]{2,1,0:T(4,128)(2,1)S(1)} %shard_map.167), channel_id=1, replica_groups=mesh['grp'=2,'chip'=8,'core'=2] {'chip'}, dimensions={0} | all-to-all | bytes 262144 | tf_op jit(solution)/shard_map/all_to_all | solution.py:40
  17.3 0.0 copy-start.2
  17.4 0.0 copy-start.10
  17.4 0.0 copy-start.12
  17.4 0.8 %shard_map.168 = bf16[8,2,4,512]{3,2,1,0:T(4,128)(2,1)S(1)} custom-call(bf16[8,4,2048]{2,1,0:T(4,128)(2,1)S(1)} %all_to_all.25.all_ref.tokens_ref, f32[1,2048]{1,0:T(1,128)S(1)} %bitcast.16, bf16[2048,128]{1,0:T(8,128)(2,1)S(1)} %copy-done.3, bf16[2048,128]{1,0:T(8,128)(2,1)S(1)} %collective-permute-done.1.refs_1_, bf16[2048,128]{1,0:T(8,128)(2,1)S(1)} %copy-done.4, ...), custom_call_target="tpu_custom_call" | custom-call | flops 10000000000 | tf_op jit(solution)/shard_map/pallas_call | solution.py:24
  18.2 9.5 %all_to_all.26 = bf16[8,2,4,512]{3,2,1,0:T(4,128)(2,1)S(1)} all-to-all(bf16[8,2,4,512]{3,2,1,0:T(4,128)(2,1)S(1)} %shard_map.168), channel_id=1, replica_groups=mesh['grp'=2,'chip'=8,'core'=2] {'chip'}, dimensions={0} | all-to-all | bytes 131072 | tf_op jit(solution)/shard_map/all_to_all | solution.py:40
  27.8 0.0 copy-start.7
  27.8 1.7 %shard_map.169 = (bf16[8,4,2048]{2,1,0:T(4,128)(2,1)S(1)}, f32[3,64,128]{2,1,0:T(8,128)S(1)}) custom-call(bf16[16,4,512]{2,1,0:T(4,128)(2,1)S(1)} %bitcast.7, f32[4,16,128,128]{3,2,1,0:T(8,128)S(1)} %copy-done.2, f32[16,128]{1,0:T(8,128)S(1)} %bitcast.17, f32[1,128]{1,0:T(1,128)S(1)} %bitcast.19), custom_call_target="tpu_custom_call" | custom-call | flops 10000000000 | tf_op jit(solution)/shard_map/pallas_call | solution.py:24
  29.4 9.7 %all_to_all.27.all_ref = bf16[8,4,2048]{2,1,0:T(4,128)(2,1)S(1)} all-to-all(bf16[8,4,2048]{2,1,0:T(4,128)(2,1)S(1)} %get-tuple-element.12), channel_id=1, replica_groups=mesh['grp'=2,'chip'=8,'core'=2] {'chip'}, dimensions={0} | all-to-all | bytes 262144 | tf_op jit(solution)/shard_map/all_to_all | solution.py:40
  39.2 0.0 slice-start.4
  39.2 0.3 shard_map.170
  39.5 0.0 slice-start.1
  39.5 0.0 slice-start.3
  39.5 0.0 slice-start.5
  39.5 10.3 %all_to_all.28.mixer_ref = bf16[8,2,32,128]{3,2,1,0:T(8,128)(2,1)S(1)} all-to-all(bf16[8,2,32,128]{3,2,1,0:T(8,128)(2,1)S(1)} %shard_map.170), channel_id=1, replica_groups=mesh['grp'=2,'chip'=8,'core'=2] {'chip'}, dimensions={0} | all-to-all | bytes 262144 | tf_op jit(solution)/shard_map/all_to_all | solution.py:40
  49.8 0.2 shard_map.171
  50.0 0.1 collective-permute-start.5
  50.1 1.3 %collective-permute-done.5.other_ref = bf16[32,2048]{1,0:T(8,128)(2,1)S(1)} collective-permute-done((bf16[32,2048]{1,0:T(8,128)(2,1)S(1)}, bf16[32,2048]{1,0:T(8,128)(2,1)S(1)}, u32[]{:S(2)}, u32[]{:S(2)}) %collective-permute-start.5) | collective-permute-done | bytes 131104 | tf_op jit(solution)/shard_map/ppermute | solution.py:44
  51.5 0.0 copy-start
  51.5 0.0 copy-start.1
  51.5 5.3 %experts.1 = (f32[8,4,2048]{2,1,0:T(4,128)S(1)}, bf16[8,4,2048]{2,1,0:T(4,128)(2,1)S(1)}, f32[4,16,128,128]{3,2,1,0:T(8,128)}) custom-call(bf16[32,2048]{1,0:T(8,128)(2,1)S(1)} %get-tuple-element.15.mine_ref, bf16[32,2048]{1,0:T(8,128)(2,1)S(1)} %collective-permute-done.5.other_ref, bf16[2048,1792]{1,0:T(8,128)(2,1)S(1)} %bitcast.11, ...), custom_call_target="tpu_custom_call" | custom-call | flops 10000000000 | tf_op jit(solution)/shard_map/experts/pallas_call | solution.py:276
  56.8 0.2 collective-permute-start.6
  57.0 1.2 %collective-permute-done.6.came_ref = bf16[8,4,2048]{2,1,0:T(4,128)(2,1)S(1)} collective-permute-done((bf16[8,4,2048]{2,1,0:T(4,128)(2,1)S(1)}, bf16[8,4,2048]{2,1,0:T(4,128)(2,1)S(1)}, u32[]{:S(2)}, u32[]{:S(2)}) %collective-permute-start.6) | collective-permute-done | bytes 131104 | tf_op jit(solution)/shard_map/ppermute | solution.py:44
  58.2 0.1 shard_map.172
  58.3 10.0 %all_to_all.29.returned_ref = bf16[8,4,2048]{2,1,0:T(4,128)(2,1)S(1)} all-to-all(bf16[8,4,2048]{2,1,0:T(4,128)(2,1)S(1)} %shard_map.172), channel_id=1, replica_groups=mesh['grp'=2,'chip'=8,'core'=2] {'chip'}, dimensions={0} | all-to-all | bytes 262144 | tf_op jit(solution)/shard_map/all_to_all | solution.py:40
  68.3 0.8 %shard_map.173 = bf16[4,2048]{1,0:T(4,128)(2,1)} custom-call(f32[8,4,2048]{2,1,0:T(4,128)S(1)} %get-tuple-element.14.middle_ref, bf16[8,4,2048]{2,1,0:T(4,128)(2,1)S(1)} %all_to_all.29.returned_ref, s32[2,4]{1,0:T(2,128)S(1)} %bitcast.8, bf16[2,4]{1,0:T(2,128)(2,1)S(1)} %bitcast.9), custom_call_target="tpu_custom_call" | custom-call | tf_op jit(solution)/shard_map/pallas_call | solution.py:24
  (36 shorter events, 0.1 us)
Async XLA Ops:
  0.6 16.7 %copy-start.3 = (bf16[2048,128]{1,0:T(8,128)(2,1)S(1)}, bf16[2048,128]{1,0:T(8,128)(2,1)}, u32[]{:S(2)}) copy-start(bf16[2048,128]{1,0:T(8,128)(2,1)} %refs_0_.1) | copy-start | bytes 1572868
  0.6 16.7 %copy-start.4 = (bf16[2048,128]{1,0:T(8,128)(2,1)S(1)}, bf16[2048,128]{1,0:T(8,128)(2,1)}, u32[]{:S(2)}) copy-start(bf16[2048,128]{1,0:T(8,128)(2,1)} %refs_2_.1) | copy-start | bytes 1572868
  0.7 16.7 %copy-start.5 = (bf16[2048,128]{1,0:T(8,128)(2,1)S(1)}, bf16[2048,128]{1,0:T(8,128)(2,1)}, u32[]{:S(2)}) copy-start(bf16[2048,128]{1,0:T(8,128)(2,1)} %refs_4_.1) | copy-start | bytes 1572868
  0.7 16.7 %copy-start.6 = (bf16[2048,128]{1,0:T(8,128)(2,1)S(1)}, bf16[2048,128]{1,0:T(8,128)(2,1)}, u32[]{:S(2)}) copy-start(bf16[2048,128]{1,0:T(8,128)(2,1)} %refs_6_.1) | copy-start | bytes 1572868
  0.7 16.6 %collective-permute-start.1 = (bf16[2048,128]{1,0:T(8,128)(2,1)}, bf16[2048,128]{1,0:T(8,128)(2,1)S(1)}, u32[]{:S(2)}, u32[]{:S(2)}) collective-permute-start(bf16[2048,128]{1,0:T(8,128)(2,1)} %refs_0_.1), channel_id=1, source_target_pairs={{0,1},{1,0},{2,3},{3,2},{4,5},{5,4},{6,7},{7,6},{8,9},{9,8},{10,11... | collective-permute-start | bytes 1572872 | tf_op jit(solution)/shard_map/ppermute | solution.py:44
  1.2 16.0 %collective-permute-start.2 = (bf16[2048,128]{1,0:T(8,128)(2,1)}, bf16[2048,128]{1,0:T(8,128)(2,1)S(1)}, u32[]{:S(2)}, u32[]{:S(2)}) collective-permute-start(bf16[2048,128]{1,0:T(8,128)(2,1)} %refs_2_.1), channel_id=1, source_target_pairs={{0,1},{1,0},{2,3},{3,2},{4,5},{5,4},{6,7},{7,6},{8,9},{9,8},{10,11... | collective-permute-start | bytes 1572872 | tf_op jit(solution)/shard_map/ppermute | solution.py:44
  1.3 16.0 %collective-permute-start.3 = (bf16[2048,128]{1,0:T(8,128)(2,1)}, bf16[2048,128]{1,0:T(8,128)(2,1)S(1)}, u32[]{:S(2)}, u32[]{:S(2)}) collective-permute-start(bf16[2048,128]{1,0:T(8,128)(2,1)} %refs_4_.1), channel_id=1, source_target_pairs={{0,1},{1,0},{2,3},{3,2},{4,5},{5,4},{6,7},{7,6},{8,9},{9,8},{10,11... | collective-permute-start | bytes 1572872 | tf_op jit(solution)/shard_map/ppermute | solution.py:44
  1.7 15.5 %collective-permute-start.4 = (bf16[2048,128]{1,0:T(8,128)(2,1)}, bf16[2048,128]{1,0:T(8,128)(2,1)S(1)}, u32[]{:S(2)}, u32[]{:S(2)}) collective-permute-start(bf16[2048,128]{1,0:T(8,128)(2,1)} %refs_6_.1), channel_id=1, source_target_pairs={{0,1},{1,0},{2,3},{3,2},{4,5},{5,4},{6,7},{7,6},{8,9},{9,8},{10,11... | collective-permute-start | bytes 1572872 | tf_op jit(solution)/shard_map/ppermute | solution.py:44
  1.8 15.4 %collective-permute-start = (bf16[2048,128]{1,0:T(8,128)(2,1)}, bf16[2048,128]{1,0:T(8,128)(2,1)S(1)}, u32[]{:S(2)}, u32[]{:S(2)}) collective-permute-start(bf16[2048,128]{1,0:T(8,128)(2,1)} %own_ref.1), channel_id=1, source_target_pairs={{0,1},{1,0},{2,3},{3,2},{4,5},{5,4},{6,7},{7,6},{8,9},{9,8},{10,11... | collective-permute-start | bytes 1572872 | tf_op jit(solution)/shard_map/ppermute | solution.py:44
  2.3 0.7 %copy-start.8 = (bf16[4,2048]{1,0:T(4,128)(2,1)S(1)}, bf16[4,2048]{1,0:T(4,128)(2,1)}, u32[]{:S(2)}) copy-start(bf16[4,2048]{1,0:T(4,128)(2,1)} %rows_ref.1) | copy-start | bytes 49156
  3.0 14.4 %copy-start.9 = (f32[2048]{0:T(1024)S(1)}, f32[2048]{0:T(1024)}, u32[]{:S(2)}) copy-start(f32[2048]{0:T(1024)} %param.20) | copy-start | bytes 24580
  17.3 10.4 %copy-start.2 = (f32[4,16,128,128]{3,2,1,0:T(8,128)S(1)}, f32[4,16,128,128]{3,2,1,0:T(8,128)}, u32[]{:S(2)}) copy-start(f32[4,16,128,128]{3,2,1,0:T(8,128)} %state_ref.3) | copy-start | bytes 12582916
  17.4 10.4 %copy-start.10 = (f32[2048]{0:T(1024)S(1)}, f32[2048]{0:T(1024)}, u32[]{:S(2)}) copy-start(f32[2048]{0:T(1024)} %param.25) | copy-start | bytes 24580
  17.4 10.4 %copy-start.12 = (f32[128]{0:T(128)S(1)}, f32[128]{0:T(128)}, u32[]{:S(2)}) copy-start(f32[128]{0:T(128)} %param.26) | copy-start | bytes 1540
  27.8 11.4 %copy-start.7 = (bf16[2048,128]{1,0:T(8,128)(2,1)S(1)}, bf16[2048,128]{1,0:T(8,128)(2,1)}, u32[]{:S(2)}) copy-start(bf16[2048,128]{1,0:T(8,128)(2,1)} %own_ref.1) | copy-start | bytes 1572868
  39.2 10.6 %copy-start.11 = (f32[2048]{0:T(1024)S(1)}, f32[2048]{0:T(1024)}, u32[]{:S(2)}) copy-start(f32[2048]{0:T(1024)} %param.28) | copy-start | bytes 24580
  39.2 12.2 %slice-start = ((s8[7340032]{0:T(1024)(128)(4,1)}), s8[4194304]{0:T(1024)(128)(4,1)S(1)}, s32[]{:S(2)}) async-start(s8[7340032]{0:T(1024)(128)(4,1)} %bitcast.10), calls=%async_computation.5 | async-start | bytes 8388608
  39.2 12.2 %slice-start.2 = ((s8[7340032]{0:T(1024)(128)(4,1)}), s8[4194304]{0:T(1024)(128)(4,1)S(1)}, s32[]{:S(2)}) async-start(s8[7340032]{0:T(1024)(128)(4,1)} %bitcast.12), calls=%async_computation.7 | async-start | bytes 8388608
  39.2 12.2 %slice-start.4 = ((s8[7340032]{0:T(1024)(128)(4,1)}), s8[4194304]{0:T(1024)(128)(4,1)S(1)}, s32[]{:S(2)}) async-start(s8[7340032]{0:T(1024)(128)(4,1)} %bitcast.14), calls=%async_computation.9 | async-start | bytes 8388608
  39.5 11.9 %slice-start.1 = ((s8[7340032]{0:T(1024)(128)(4,1)}), s8[3145728]{0:T(1024)(128)(4,1)S(1)}, s32[]{:S(2)}) async-start(s8[7340032]{0:T(1024)(128)(4,1)} %bitcast.10), calls=%async_computation.6 | async-start | bytes 6291456
  39.5 11.9 %slice-start.3 = ((s8[7340032]{0:T(1024)(128)(4,1)}), s8[3145728]{0:T(1024)(128)(4,1)S(1)}, s32[]{:S(2)}) async-start(s8[7340032]{0:T(1024)(128)(4,1)} %bitcast.12), calls=%async_computation.8 | async-start | bytes 6291456
  39.5 11.9 %slice-start.5 = ((s8[7340032]{0:T(1024)(128)(4,1)}), s8[3145728]{0:T(1024)(128)(4,1)S(1)}, s32[]{:S(2)}) async-start(s8[7340032]{0:T(1024)(128)(4,1)} %bitcast.14), calls=%async_computation.10 | async-start | bytes 6291456
  50.0 1.4 %collective-permute-start.5 = (bf16[32,2048]{1,0:T(8,128)(2,1)S(1)}, bf16[32,2048]{1,0:T(8,128)(2,1)S(1)}, u32[]{:S(2)}, u32[]{:S(2)}) collective-permute-start(bf16[32,2048]{1,0:T(8,128)(2,1)S(1)} %get-tuple-element.15.mine_ref), channel_id=1, source_target_pairs={{0,1},{1,0},{2,3},{3,2},{4,5},{5,4},{6,7},{7,6},{8,9},{9,8},{10,11... | collective-permute-start | bytes 393224 | tf_op jit(solution)/shard_map/ppermute | solution.py:44
  51.5 16.8 %copy-start = (s32[4,2]{0,1:T(2,128)S(1)}, s32[4,2]{0,1:T(2,128)}, u32[]{:S(2)}) copy-start(s32[4,2]{0,1:T(2,128)} %param.18) | copy-start | bytes 100
  51.5 16.8 %copy-start.1 = (bf16[4,2]{0,1:T(2,128)(2,1)S(1)}, bf16[4,2]{0,1:T(2,128)(2,1)}, u32[]{:S(2)}) copy-start(bf16[4,2]{0,1:T(2,128)(2,1)} %param.19) | copy-start | bytes 52
  56.8 1.4 %collective-permute-start.6 = (bf16[8,4,2048]{2,1,0:T(4,128)(2,1)S(1)}, bf16[8,4,2048]{2,1,0:T(4,128)(2,1)S(1)}, u32[]{:S(2)}, u32[]{:S(2)}) collective-permute-start(bf16[8,4,2048]{2,1,0:T(4,128)(2,1)S(1)} %get-tuple-element.18), channel_id=1, source_target_pairs={{0,1},{1,0},{2,3},{3,2},{4,5},{5,4},{6,7},{7,6},{8,9},{9,8},{10,11... | collective-permute-start | bytes 393224 | tf_op jit(solution)/shard_map/ppermute | solution.py:44

commit v3 on v2

--- a/solution.py
+++ b/solution.py
@@ -54,7 +54,11 @@
         target[i * rows : (i + 1) * rows, :] = source[i].astype(f32)
 
 
-def spread_body(rows_ref, out_ref):
+def mark_body(out_ref):
+    out_ref[...] = jnp.zeros(out_ref.shape, out_ref.dtype)
+
+
+def spread_body(rows_ref, mark_ref, out_ref):
     for i in range(out_ref.shape[0]):
         out_ref[i] = rows_ref[...]
 
@@ -72,6 +76,18 @@
         for chip in range(all_ref.shape[0]):
             block = product[chip * rows : (chip + 1) * rows, :].astype(bf16)
             out_ref[chip, side, :, p * cols : (p + 1) * cols] = block
+
+
+def thirds(values):
+    first = values.astype(bf16).astype(f32)
+    second = (values - first).astype(bf16).astype(f32)
+    return first, second, (values - first - second).astype(bf16).astype(f32)
+
+
+def chooser(count, dim):
+    shape = (3 * count, count * dim)
+    row, column = lax.broadcasted_iota(jnp.int32, shape, 0), lax.broadcasted_iota(jnp.int32, shape, 1)
+    return (row % count == column // dim).astype(f32)
 
 
 def mixer_body(owned_ref, state_ref, bound_ref, gain_ref, out_ref, gates_ref, raw_ref, bounds_ref, read_ref):
@@ -88,12 +104,16 @@
     gates_ref[0] = decay
     gates_ref[1] = key_vec
     gates_ref[2] = input_raw
-    weights = query_vec * decay
-    for start in range(0, heads * rows, 8):
-        columns = weights[start : start + 8, :].T
-        for p in range(start, min(start + 8, heads * rows)):
-            column = columns[:, p - start : p - start + 1]
-            read_ref[p : p + 1, :] = jnp.sum(column * state_ref[p % rows, p // rows], axis=0, keepdims=True)
+    weights = thirds(query_vec * decay)
+    take = min(16, heads * rows)
+    chosen = chooser(take, dim).astype(bf16)
+    for start in range(0, heads * rows, take):
+        columns = jnp.concatenate([part[start : start + take, :] for part in weights], axis=0).T
+        wide = jnp.dot(columns.astype(bf16), chosen, preferred_element_type=f32)
+        for j in range(take):
+            h, t = divmod(start + j, rows)
+            product = wide[:, j * dim : (j + 1) * dim] * state_ref[t, h]
+            read_ref[start + j : start + j + 1, :] = jnp.sum(product, axis=0, keepdims=True)
     read = read_ref[...] + jnp.sum(query_vec * key_vec, axis=-1, keepdims=True) * input_raw
     mixed = rms(read) * gain_ref[...] * (gate_raw * jax.nn.sigmoid(gate_raw))
     for h in range(heads):
@@ -143,7 +163,9 @@
     chips, rows = keep_ref.shape[:2]
     half = mine_ref.shape[0]
     hidden_cols, width = gate_ref.shape[1], down_ref.shape[1]
-    seqs, heads = state_ref.shape[:2]
+    seqs, heads, dim = state_ref.shape[:3]
+    step_heads = max(1, 8 // seqs)
+    take, groups = step_heads * seqs, heads // step_heads
     step = 2 * LANES
     blocks = [pl.ds(i, min(step, hidden_cols - i)) for i in range(0, hidden_cols, step)]
     parts = [pl.ds(i, min(step, width - i)) for i in range(0, width, step)]
@@ -152,19 +174,26 @@
     normed = normed_ref[...]
     copies = []
 
-    def renew(h):
-        group = slice(h * seqs, (h + 1) * seqs)
-        decay, key_vec, value = gates_ref[0, group, :].T, gates_ref[1, group, :].T, gates_ref[2, group, :]
-        for t in range(seqs):
-            held_ref[t, h] = decay[:, t : t + 1] * state_ref[t, h] + key_vec[:, t : t + 1] * value[t : t + 1, :]
-        copies.append(pltpu.make_async_copy(held_ref.at[:, h], new_ref.at[:, h], sems.at[h]))
+    chosen = chooser(take, dim)
+
+    def renew(g):
+        group = slice(g * take, (g + 1) * take)
+        decay, key_vec, value = gates_ref[0, group, :].T, thirds(gates_ref[1, group, :]), gates_ref[2, group, :]
+        columns = jnp.concatenate(key_vec, axis=0).T.astype(bf16)
+        values = jnp.concatenate([jnp.concatenate([value] * 3, axis=0)] * take, axis=1) * chosen
+        outer = jnp.dot(columns, values.astype(bf16), preferred_element_type=f32)
+        for j in range(take):
+            h, t = divmod(g * take + j, seqs)
+            held_ref[t, h] = decay[:, j : j + 1] * state_ref[t, h] + outer[:, j * dim : (j + 1) * dim]
+        part = pl.ds(g * step_heads, step_heads)
+        copies.append(pltpu.make_async_copy(held_ref.at[:, part], new_ref.at[:, part], sems.at[g]))
         copies[-1].start()
 
     for i, block in enumerate(blocks):
         gate_act = jnp.dot(normed, gate_ref[:, block], preferred_element_type=f32)
         up_act = jnp.dot(normed, up_ref[:, block], preferred_element_type=f32)
-        for h in range(i * heads // len(blocks), (i + 1) * heads // len(blocks)):
-            renew(h)
+        for g in range(i * groups // len(blocks), (i + 1) * groups // len(blocks)):
+            renew(g)
         hidden_ref[:, block] = (gate_act * jax.nn.sigmoid(gate_act) * up_act).astype(bf16)
     hidden = hidden_ref[...]
     for part in parts:
@@ -229,7 +258,8 @@
     weights = []
     for weight in (w_query, w_forget, w_input, w_gate, w_out):
         weights += [weight, swap(weight)]
-    sent = call(spread_body, full, (tokens,), 4, flops=COST)
+    mark = call(mark_body, shape((8, LANES), f32), (), 1, flops=COST)
+    sent = call(spread_body, full, (tokens, mark), 4, flops=COST)
     all_tokens = exchange(sent)
     all_tokens, out_cross = lax.optimization_barrier((all_tokens, weights[9]))
     projected = call(
@@ -238,7 +268,6 @@
         (all_tokens, norm_mix.reshape(1, width), *weights[:8]),
         8,
         scratch=rows_scratch,
-        flops=COST,
     )
     owned = exchange(projected).reshape(2 * chips, rows, 4 * cols)
     if cols != dim:
@@ -249,7 +278,6 @@
         [full, shape((3, heads * rows, dim), f32)],
         (owned, state, lower_bound.reshape(heads, dim), head_gain.reshape(1, dim)),
         12,
-        flops=COST,
         scratch=[
             pltpu.VMEM((heads * rows, 4 * dim), f32),
             pltpu.VMEM((heads * rows, dim), f32),
@@ -257,19 +285,13 @@
         ],
     )
     mixer_cols = call(
-        out_body,
-        shape((chips, 2, half, cols), bf16),
-        (exchange(mixed), w_out, out_cross),
-        6,
-        flops=COST,
-        scratch=rows_scratch,
+        out_body, shape((chips, 2, half, cols), bf16), (exchange(mixed), w_out, out_cross), 6, scratch=rows_scratch
     )
     normed, middle = call(
         norm_body,
         [shape((half, width), bf16), shape((chips, rows, width), f32)],
         (all_tokens, exchange(mixer_cols), norm_ffn.reshape(1, width)),
         6,
-        flops=COST,
         scratch=rows_scratch,
     )
     vmem = pl.BlockSpec(memory_space=pltpu.VMEM)

time: 69.4 us -> 67 us (0.965)
  Pallas kernels: 9.09 us -> 7.81 us
  local copies, waits for them, and re-layouts: 0.82 us -> 0.11 us
    pallas_call x7 -> x8, Pallas kernels: 3.79 us -> 3.03 us  [call(): pl.pallas_call(body, out_shape=outs, in_specs=[pl.BlockSpec(memory_space=...]
    unnamed x38, local copies, waits for them, and re-layouts: 0.82 us -> 0.11 us
where the time goes in v3:
time: 67 us; the launch traced here: 66.7 us
  blocking collectives  53.4 us (80%)
  Pallas kernels  7.81 us (12%)
  waiting for transfers between devices  2.56 us (4%)
  starting transfers between devices  1.85 us (3%)
  between operations  0.94 us (1%)
    all_to_all x5, blocking collectives, exchange(): lax.all_to_all(chunks, 'chip', split_axis=0, concat_axis=0, tiled=True)  53.4 us
    pallas_call x1, Pallas kernels, body(): pl.pallas_call(expert_body, out_shape=[shape((chips, rows, width), f32),...  4.77 us
    pallas_call x8, Pallas kernels, call(): pl.pallas_call(body, out_shape=outs, in_specs=[pl.BlockSpec(memory_space=...  3.03 us
    ppermute x7, waiting for transfers between devices, swap(): return lax.ppermute(values, 'core', [(0, 1), (1, 0)])  2.56 us
    ppermute x7, starting transfers between devices, swap(): return lax.ppermute(values, 'core', [(0, 1), (1, 0)])  1.85 us
  transfers between devices with their start and end apart: 7, of which 2 were waited for; matrix products, arithmetic and copies ran while one was open for 0% of the time, Pallas kernels for 0%

profile of v3, /device:TPU:0, one launch (start us, length us, event | category | flops | bytes accessed | tf_op | source)
XLA Modules:
  0.0 66.7 jit_solution(16492775492454628941)
XLA Ops:
  0.6 0.6 collective-permute-start.1
  1.2 0.1 collective-permute-start.2
  1.3 0.4 collective-permute-start.3
  1.7 0.1 collective-permute-start.4
  1.8 0.4 collective-permute-start
  2.2 0.0 copy-start.1
  2.3 0.0 copy-start.2
  2.3 0.0 copy-start.3
  2.3 0.0 copy-start.6
  2.3 0.0 copy-start.7
  2.3 0.0 slice-start.1
  2.3 0.0 slice-start.3
  2.4 0.0 slice-start.5
  2.4 0.0 copy-start
  2.4 0.0 copy-start.5
  2.4 14.5 %all_to_all.25.all_ref.tokens_ref = bf16[8,4,2048]{2,1,0:T(4,128)(2,1)S(1)} all-to-all(bf16[8,4,2048]{2,1,0:T(4,128)(2,1)S(1)} %shard_map.168), channel_id=1, replica_groups=mesh['grp'=2,'chip'=8,'core'=2] {'chip'}, dimensions={0} | all-to-all | bytes 262144 | tf_op jit(solution)/shard_map/all_to_all | solution.py:40
  17.0 0.8 %shard_map.169 = bf16[8,2,4,512]{3,2,1,0:T(4,128)(2,1)S(1)} custom-call(bf16[8,4,2048]{2,1,0:T(4,128)(2,1)S(1)} %all_to_all.25.all_ref.tokens_ref, f32[1,2048]{1,0:T(1,128)S(1)} %bitcast.8, bf16[2048,128]{1,0:T(8,128)(2,1)S(1)} %copy-done.1, bf16[2048,128]{1,0:T(8,128)(2,1)S(1)} %collective-permute-done.1.refs_1_, bf16[2048,128]{1,0:T(8,128)(2,1)S(1)} %copy-done.2, ...), custom_call_target="tpu_custom_call" | custom-call | tf_op jit(solution)/shard_map/pallas_call | solution.py:24
  17.9 9.4 %all_to_all.26 = bf16[8,2,4,512]{3,2,1,0:T(4,128)(2,1)S(1)} all-to-all(bf16[8,2,4,512]{3,2,1,0:T(4,128)(2,1)S(1)} %shard_map.169), channel_id=1, replica_groups=mesh['grp'=2,'chip'=8,'core'=2] {'chip'}, dimensions={0} | all-to-all | bytes 131072 | tf_op jit(solution)/shard_map/all_to_all | solution.py:40
  27.3 0.9 %shard_map.170 = (bf16[8,4,2048]{2,1,0:T(4,128)(2,1)S(1)}, f32[3,64,128]{2,1,0:T(8,128)S(1)}) custom-call(bf16[16,4,512]{2,1,0:T(4,128)(2,1)S(1)} %bitcast.7, f32[4,16,128,128]{3,2,1,0:T(8,128)S(1)} %copy-done, f32[16,128]{1,0:T(8,128)S(1)} %bitcast.9, f32[1,128]{1,0:T(1,128)S(1)} %bitcast.12), custom_call_target="tpu_custom_call" | custom-call | tf_op jit(solution)/shard_map/pallas_call | solution.py:24
  28.2 9.7 %all_to_all.27.all_ref = bf16[8,4,2048]{2,1,0:T(4,128)(2,1)S(1)} all-to-all(bf16[8,4,2048]{2,1,0:T(4,128)(2,1)S(1)} %get-tuple-element.12), channel_id=1, replica_groups=mesh['grp'=2,'chip'=8,'core'=2] {'chip'}, dimensions={0} | all-to-all | bytes 262144 | tf_op jit(solution)/shard_map/all_to_all | solution.py:40
  37.9 0.3 shard_map.171
  38.2 9.7 %all_to_all.28.mixer_ref = bf16[8,2,32,128]{3,2,1,0:T(8,128)(2,1)S(1)} all-to-all(bf16[8,2,32,128]{3,2,1,0:T(8,128)(2,1)S(1)} %shard_map.171), channel_id=1, replica_groups=mesh['grp'=2,'chip'=8,'core'=2] {'chip'}, dimensions={0} | all-to-all | bytes 262144 | tf_op jit(solution)/shard_map/all_to_all | solution.py:40
  48.0 0.2 shard_map.172
  48.2 0.1 collective-permute-start.5
  48.2 1.3 %collective-permute-done.5.other_ref = bf16[32,2048]{1,0:T(8,128)(2,1)S(1)} collective-permute-done((bf16[32,2048]{1,0:T(8,128)(2,1)S(1)}, bf16[32,2048]{1,0:T(8,128)(2,1)S(1)}, u32[]{:S(2)}, u32[]{:S(2)}) %collective-permute-start.5) | collective-permute-done | bytes 131104 | tf_op jit(solution)/shard_map/ppermute | solution.py:44
  49.6 0.0 copy-start.9
  49.7 4.8 %experts.1 = (f32[8,4,2048]{2,1,0:T(4,128)S(1)}, bf16[8,4,2048]{2,1,0:T(4,128)(2,1)S(1)}, f32[4,16,128,128]{3,2,1,0:T(8,128)}) custom-call(bf16[32,2048]{1,0:T(8,128)(2,1)S(1)} %get-tuple-element.15.mine_ref, bf16[32,2048]{1,0:T(8,128)(2,1)S(1)} %collective-permute-done.5.other_ref, bf16[2048,1792]{1,0:T(8,128)(2,1)S(1)} %bitcast.15, ...), custom_call_target="tpu_custom_call" | custom-call | flops 10000000000 | tf_op jit(solution)/shard_map/experts/pallas_call | solution.py:298
  54.4 0.2 collective-permute-start.6
  54.6 1.2 %collective-permute-done.6.came_ref = bf16[8,4,2048]{2,1,0:T(4,128)(2,1)S(1)} collective-permute-done((bf16[8,4,2048]{2,1,0:T(4,128)(2,1)S(1)}, bf16[8,4,2048]{2,1,0:T(4,128)(2,1)S(1)}, u32[]{:S(2)}, u32[]{:S(2)}) %collective-permute-start.6) | collective-permute-done | bytes 131104 | tf_op jit(solution)/shard_map/ppermute | solution.py:44
  55.9 0.1 shard_map.173
  55.9 10.0 %all_to_all.29.returned_ref = bf16[8,4,2048]{2,1,0:T(4,128)(2,1)S(1)} all-to-all(bf16[8,4,2048]{2,1,0:T(4,128)(2,1)S(1)} %shard_map.173), channel_id=1, replica_groups=mesh['grp'=2,'chip'=8,'core'=2] {'chip'}, dimensions={0} | all-to-all | bytes 262144 | tf_op jit(solution)/shard_map/all_to_all | solution.py:40
  65.9 0.8 %shard_map.174 = bf16[4,2048]{1,0:T(4,128)(2,1)} custom-call(f32[8,4,2048]{2,1,0:T(4,128)S(1)} %get-tuple-element.14.middle_ref, bf16[8,4,2048]{2,1,0:T(4,128)(2,1)S(1)} %all_to_all.29.returned_ref, s32[2,4]{1,0:T(2,128)S(1)} %bitcast.11, bf16[2,4]{1,0:T(2,128)(2,1)S(1)} %bitcast.13), custom_call_target="tpu_custom_call" | custom-call | tf_op jit(solution)/shard_map/pallas_call | solution.py:24
  (37 shorter events, 0.1 us)
Async XLA Ops:
  0.6 1.6 %copy-start.12 = (bf16[4,2048]{1,0:T(4,128)(2,1)S(1)}, bf16[4,2048]{1,0:T(4,128)(2,1)}, u32[]{:S(2)}) copy-start(bf16[4,2048]{1,0:T(4,128)(2,1)} %rows_ref.1) | copy-start | bytes 49156
  0.6 16.3 %collective-permute-start.1 = (bf16[2048,128]{1,0:T(8,128)(2,1)}, bf16[2048,128]{1,0:T(8,128)(2,1)S(1)}, u32[]{:S(2)}, u32[]{:S(2)}) collective-permute-start(bf16[2048,128]{1,0:T(8,128)(2,1)} %refs_0_.1), channel_id=1, source_target_pairs={{0,1},{1,0},{2,3},{3,2},{4,5},{5,4},{6,7},{7,6},{8,9},{9,8},{10,11... | collective-permute-start | bytes 1572872 | tf_op jit(solution)/shard_map/ppermute | solution.py:44
  1.2 15.8 %collective-permute-start.2 = (bf16[2048,128]{1,0:T(8,128)(2,1)}, bf16[2048,128]{1,0:T(8,128)(2,1)S(1)}, u32[]{:S(2)}, u32[]{:S(2)}) collective-permute-start(bf16[2048,128]{1,0:T(8,128)(2,1)} %refs_2_.1), channel_id=1, source_target_pairs={{0,1},{1,0},{2,3},{3,2},{4,5},{5,4},{6,7},{7,6},{8,9},{9,8},{10,11... | collective-permute-start | bytes 1572872 | tf_op jit(solution)/shard_map/ppermute | solution.py:44
  1.3 15.7 %collective-permute-start.3 = (bf16[2048,128]{1,0:T(8,128)(2,1)}, bf16[2048,128]{1,0:T(8,128)(2,1)S(1)}, u32[]{:S(2)}, u32[]{:S(2)}) collective-permute-start(bf16[2048,128]{1,0:T(8,128)(2,1)} %refs_4_.1), channel_id=1, source_target_pairs={{0,1},{1,0},{2,3},{3,2},{4,5},{5,4},{6,7},{7,6},{8,9},{9,8},{10,11... | collective-permute-start | bytes 1572872 | tf_op jit(solution)/shard_map/ppermute | solution.py:44
  1.7 15.3 %collective-permute-start.4 = (bf16[2048,128]{1,0:T(8,128)(2,1)}, bf16[2048,128]{1,0:T(8,128)(2,1)S(1)}, u32[]{:S(2)}, u32[]{:S(2)}) collective-permute-start(bf16[2048,128]{1,0:T(8,128)(2,1)} %refs_6_.1), channel_id=1, source_target_pairs={{0,1},{1,0},{2,3},{3,2},{4,5},{5,4},{6,7},{7,6},{8,9},{9,8},{10,11... | collective-permute-start | bytes 1572872 | tf_op jit(solution)/shard_map/ppermute | solution.py:44
  1.8 15.2 %collective-permute-start = (bf16[2048,128]{1,0:T(8,128)(2,1)}, bf16[2048,128]{1,0:T(8,128)(2,1)S(1)}, u32[]{:S(2)}, u32[]{:S(2)}) collective-permute-start(bf16[2048,128]{1,0:T(8,128)(2,1)} %own_ref.1), channel_id=1, source_target_pairs={{0,1},{1,0},{2,3},{3,2},{4,5},{5,4},{6,7},{7,6},{8,9},{9,8},{10,11... | collective-permute-start | bytes 1572872 | tf_op jit(solution)/shard_map/ppermute | solution.py:44
  2.2 47.4 %slice-start = ((s8[7340032]{0:T(1024)(128)(4,1)}), s8[4194304]{0:T(1024)(128)(4,1)S(1)}, s32[]{:S(2)}) async-start(s8[7340032]{0:T(1024)(128)(4,1)} %bitcast.14), calls=%async_computation.5 | async-start | bytes 8388608
  2.2 47.4 %slice-start.2 = ((s8[7340032]{0:T(1024)(128)(4,1)}), s8[4194304]{0:T(1024)(128)(4,1)S(1)}, s32[]{:S(2)}) async-start(s8[7340032]{0:T(1024)(128)(4,1)} %bitcast.16), calls=%async_computation.7 | async-start | bytes 8388608
  2.2 47.4 %slice-start.4 = ((s8[7340032]{0:T(1024)(128)(4,1)}), s8[4194304]{0:T(1024)(128)(4,1)S(1)}, s32[]{:S(2)}) async-start(s8[7340032]{0:T(1024)(128)(4,1)} %bitcast.18), calls=%async_computation.9 | async-start | bytes 8388608
  2.2 14.8 %copy-start.1 = (bf16[2048,128]{1,0:T(8,128)(2,1)S(1)}, bf16[2048,128]{1,0:T(8,128)(2,1)}, u32[]{:S(2)}) copy-start(bf16[2048,128]{1,0:T(8,128)(2,1)} %refs_0_.1) | copy-start | bytes 1572868
  2.3 14.8 %copy-start.2 = (bf16[2048,128]{1,0:T(8,128)(2,1)S(1)}, bf16[2048,128]{1,0:T(8,128)(2,1)}, u32[]{:S(2)}) copy-start(bf16[2048,128]{1,0:T(8,128)(2,1)} %refs_2_.1) | copy-start | bytes 1572868
  2.3 14.7 %copy-start.3 = (bf16[2048,128]{1,0:T(8,128)(2,1)S(1)}, bf16[2048,128]{1,0:T(8,128)(2,1)}, u32[]{:S(2)}) copy-start(bf16[2048,128]{1,0:T(8,128)(2,1)} %refs_4_.1) | copy-start | bytes 1572868
  2.3 14.7 %copy-start.4 = (bf16[2048,128]{1,0:T(8,128)(2,1)S(1)}, bf16[2048,128]{1,0:T(8,128)(2,1)}, u32[]{:S(2)}) copy-start(bf16[2048,128]{1,0:T(8,128)(2,1)} %refs_6_.1) | copy-start | bytes 1572868
  2.3 14.7 %copy-start.6 = (f32[2048]{0:T(1024)S(1)}, f32[2048]{0:T(1024)}, u32[]{:S(2)}) copy-start(f32[2048]{0:T(1024)} %param.20) | copy-start | bytes 24580
  2.3 25.0 %copy-start.7 = (f32[2048]{0:T(1024)S(1)}, f32[2048]{0:T(1024)}, u32[]{:S(2)}) copy-start(f32[2048]{0:T(1024)} %param.25) | copy-start | bytes 24580
  2.3 25.0 %copy-start.10 = (f32[128]{0:T(128)S(1)}, f32[128]{0:T(128)}, u32[]{:S(2)}) copy-start(f32[128]{0:T(128)} %param.26) | copy-start | bytes 1540
  2.3 47.3 %slice-start.1 = ((s8[7340032]{0:T(1024)(128)(4,1)}), s8[3145728]{0:T(1024)(128)(4,1)S(1)}, s32[]{:S(2)}) async-start(s8[7340032]{0:T(1024)(128)(4,1)} %bitcast.14), calls=%async_computation.6 | async-start | bytes 6291456
  2.3 47.3 %slice-start.3 = ((s8[7340032]{0:T(1024)(128)(4,1)}), s8[3145728]{0:T(1024)(128)(4,1)S(1)}, s32[]{:S(2)}) async-start(s8[7340032]{0:T(1024)(128)(4,1)} %bitcast.16), calls=%async_computation.8 | async-start | bytes 6291456
  2.4 47.3 %slice-start.5 = ((s8[7340032]{0:T(1024)(128)(4,1)}), s8[3145728]{0:T(1024)(128)(4,1)S(1)}, s32[]{:S(2)}) async-start(s8[7340032]{0:T(1024)(128)(4,1)} %bitcast.18), calls=%async_computation.10 | async-start | bytes 6291456
  2.4 24.9 %copy-start = (f32[4,16,128,128]{3,2,1,0:T(8,128)S(1)}, f32[4,16,128,128]{3,2,1,0:T(8,128)}, u32[]{:S(2)}) copy-start(f32[4,16,128,128]{3,2,1,0:T(8,128)} %state_ref.3) | copy-start | bytes 12582916
  2.4 35.5 %copy-start.5 = (bf16[2048,128]{1,0:T(8,128)(2,1)S(1)}, bf16[2048,128]{1,0:T(8,128)(2,1)}, u32[]{:S(2)}) copy-start(bf16[2048,128]{1,0:T(8,128)(2,1)} %own_ref.1) | copy-start | bytes 1572868
  2.4 45.6 %copy-start.8 = (f32[2048]{0:T(1024)S(1)}, f32[2048]{0:T(1024)}, u32[]{:S(2)}) copy-start(f32[2048]{0:T(1024)} %param.28) | copy-start | bytes 24580
  48.2 1.4 %collective-permute-start.5 = (bf16[32,2048]{1,0:T(8,128)(2,1)S(1)}, bf16[32,2048]{1,0:T(8,128)(2,1)S(1)}, u32[]{:S(2)}, u32[]{:S(2)}) collective-permute-start(bf16[32,2048]{1,0:T(8,128)(2,1)S(1)} %get-tuple-element.15.mine_ref), channel_id=1, source_target_pairs={{0,1},{1,0},{2,3},{3,2},{4,5},{5,4},{6,7},{7,6},{8,9},{9,8},{10,11... | collective-permute-start | bytes 393224 | tf_op jit(solution)/shard_map/ppermute | solution.py:44
  49.6 16.2 %copy-start.9 = (s32[4,2]{0,1:T(2,128)S(1)}, s32[4,2]{0,1:T(2,128)}, u32[]{:S(2)}) copy-start(s32[4,2]{0,1:T(2,128)} %param.18) | copy-start | bytes 100
  49.6 16.2 %copy-start.11 = (bf16[4,2]{0,1:T(2,128)(2,1)S(1)}, bf16[4,2]{0,1:T(2,128)(2,1)}, u32[]{:S(2)}) copy-start(bf16[4,2]{0,1:T(2,128)(2,1)} %param.19) | copy-start | bytes 52
  54.4 1.4 %collective-permute-start.6 = (bf16[8,4,2048]{2,1,0:T(4,128)(2,1)S(1)}, bf16[8,4,2048]{2,1,0:T(4,128)(2,1)S(1)}, u32[]{:S(2)}, u32[]{:S(2)}) collective-permute-start(bf16[8,4,2048]{2,1,0:T(4,128)(2,1)S(1)} %get-tuple-element.18), channel_id=1, source_target_pairs={{0,1},{1,0},{2,3},{3,2},{4,5},{5,4},{6,7},{7,6},{8,9},{9,8},{10,11... | collective-permute-start | bytes 393224 | tf_op jit(solution)/shard_map/ppermute | solution.py:44

commit v4 on v3

--- a/solution.py
+++ b/solution.py
@@ -36,8 +36,24 @@
 AXES = ("chip", "core")
 
 
+def chip_order():
+    half = lax.axis_size("chip") // 2
+    inward = [i // 2 if i % 2 == 0 else half - 1 - i // 2 for i in range(half)]
+    return [2 * i + odd for odd in range(2) for i in inward]
+
+
+def my_place():
+    chip, half = lax.axis_index("chip"), lax.axis_size("chip") // 2
+    i = chip // 2
+    return (chip % 2) * half + jnp.where(2 * i < half, 2 * i, 2 * (half - 1 - i) + 1)
+
+
+def lines():
+    return [[2 * chip + (line ^ chip % 2) for chip in chip_order()] for line in range(2)]
+
+
 def exchange(chunks):
-    return lax.all_to_all(chunks, "chip", split_axis=0, concat_axis=0, tiled=True)
+    return lax.all_to_all(chunks, AXES, split_axis=0, concat_axis=0, axis_index_groups=lines(), tiled=True)
 
 
 def swap(values):
@@ -90,11 +106,11 @@
     return (row % count == column // dim).astype(f32)
 
 
-def mixer_body(owned_ref, state_ref, bound_ref, gain_ref, out_ref, gates_ref, raw_ref, bounds_ref, read_ref):
+def mixer_body(source, owned_ref, state_ref, bound_ref, gain_ref, out_ref, gates_ref, raw_ref, bounds_ref, read_ref):
     heads, rows = owned_ref.shape[0], owned_ref.shape[1]
     dim = bound_ref.shape[1]
     for h in range(heads):
-        raw_ref[h * rows : (h + 1) * rows, :] = owned_ref[h].astype(f32)
+        raw_ref[h * rows : (h + 1) * rows, :] = owned_ref[source[h]].astype(f32)
         bounds_ref[h * rows : (h + 1) * rows, :] = jnp.broadcast_to(bound_ref[h : h + 1, :], (rows, dim))
     bound = bounds_ref[...]
     query_raw, forget_raw, input_raw, gate_raw = (raw_ref[:, p * dim : (p + 1) * dim] for p in range(4))
@@ -135,10 +151,10 @@
 def norm_body(tokens_ref, mixer_ref, gain_ref, normed_ref, middle_ref, rows_ref):
     rows, cols = middle_ref.shape[1], mixer_ref.shape[3]
     unpack(tokens_ref, rows_ref)
-    for chip in range(mixer_ref.shape[0]):
+    for place, chip in enumerate(chip_order()):
         for side in range(2):
             part = slice((2 * chip + side) * cols, (2 * chip + side + 1) * cols)
-            rows_ref[:, part] = rows_ref[:, part] + mixer_ref[chip, side].astype(f32)
+            rows_ref[:, part] = rows_ref[:, part] + mixer_ref[place, side].astype(f32)
     normed_ref[...] = (rms(rows_ref[...]) * gain_ref[...]).astype(bf16)
     for chip in range(middle_ref.shape[0]):
         middle_ref[chip] = rows_ref[chip * rows : (chip + 1) * rows, :]
@@ -211,7 +227,7 @@
 
 
 def final_body(group, middle_ref, returned_ref, ids_ref, weights_ref, out_ref, shares_ref):
-    total = middle_ref[lax.axis_index("chip")]
+    total = middle_ref[my_place()]
     rows = total.shape[0]
     ids, weights = ids_ref[...], weights_ref[...].astype(f32)
     shares_ref[...] = jnp.zeros(shares_ref.shape, f32)
@@ -220,9 +236,10 @@
     shares = shares_ref[...].T
     for e in range(EXPERTS):
         share = shares[:rows, e : e + 1]
-        summed = returned_ref[e * group].astype(f32)
-        for i in range(e * group + 1, (e + 1) * group):
-            summed = summed + returned_ref[i].astype(f32)
+        places = [place for place, chip in enumerate(chip_order()) if chip // group == e]
+        summed = returned_ref[places[0]].astype(f32)
+        for place in places[1:]:
+            summed = summed + returned_ref[place].astype(f32)
         total = total + share * summed
     out_ref[...] = total.astype(bf16)
 
@@ -270,11 +287,15 @@
         scratch=rows_scratch,
     )
     owned = exchange(projected).reshape(2 * chips, rows, 4 * cols)
+    order = chip_order()
+    source = [2 * order.index(chip) + side for chip in range(chips) for side in range(2)]
     if cols != dim:
+        owned = jnp.stack([owned[i] for i in source])
+        source = list(range(heads))
         owned = owned.reshape(2 * chips, rows, 4, cols).transpose(1, 2, 0, 3).reshape(rows, 4, heads, dim)
         owned = owned.transpose(2, 0, 1, 3).reshape(heads, rows, 4 * dim)
     mixed, gates = call(
-        mixer_body,
+        functools.partial(mixer_body, source),
         [full, shape((3, heads * rows, dim), f32)],
         (owned, state, lower_bound.reshape(heads, dim), head_gain.reshape(1, dim)),
         12,

time: 67 us -> 63.8 us (0.952)
  blocking collectives: 53.4 us -> 49.3 us
  starting transfers between devices: 1.85 us -> 3.01 us
    all_to_all x5, blocking collectives: 53.4 us -> 49.3 us  [exchange(): lax.all_to_all(chunks, AXES, split_axis=0, concat_axis=0, axis_index_grou...]
    ppermute x7, starting transfers between devices: 1.85 us -> 3.01 us  [swap(): return lax.ppermute(values, 'core', [(0, 1), (1, 0)])]
where the time goes in v4:
time: 63.8 us; the launch traced here: 63.1 us
  blocking collectives  49.3 us (77%)
  Pallas kernels  7.8 us (12%)
  starting transfers between devices  3.01 us (5%)
  waiting for transfers between devices  1.99 us (3%)
  between operations  0.93 us (1%)
    all_to_all x5, blocking collectives, exchange(): lax.all_to_all(chunks, AXES, split_axis=0, concat_axis=0, axis_index_grou...  49.3 us
    pallas_call x1, Pallas kernels, body(): pl.pallas_call(expert_body, out_shape=[shape((chips, rows, width), f32),...  4.77 us
    pallas_call x8, Pallas kernels, call(): pl.pallas_call(body, out_shape=outs, in_specs=[pl.BlockSpec(memory_space=...  3.03 us
    ppermute x7, starting transfers between devices, swap(): return lax.ppermute(values, 'core', [(0, 1), (1, 0)])  3.01 us
    ppermute x7, waiting for transfers between devices, swap(): return lax.ppermute(values, 'core', [(0, 1), (1, 0)])  1.99 us
  transfers between devices with their start and end apart: 7, of which 2 were waited for; matrix products, arithmetic and copies ran while one was open for 0% of the time, Pallas kernels for 0%

profile of v4, /device:TPU:0, one launch (start us, length us, event | category | flops | bytes accessed | tf_op | source)
XLA Modules:
  0.0 63.1 jit_solution(14193817333553338364)
XLA Ops:
  0.6 0.6 collective-permute-start.1
  1.2 0.1 collective-permute-start.2
  1.3 0.4 collective-permute-start.3
  1.7 0.1 collective-permute-start.4
  1.8 0.4 collective-permute-start
  2.2 0.0 copy-start.1
  2.3 0.0 copy-start.2
  2.3 0.0 copy-start.6
  2.3 0.0 copy-start.7
  2.3 0.0 slice-start.1
  2.3 0.0 slice-start.3
  2.4 0.0 slice-start.5
  2.4 0.0 copy-start
  2.4 0.0 copy-start.5
  2.4 13.8 %all_to_all.25.all_ref.tokens_ref = bf16[8,4,2048]{2,1,0:T(4,128)(2,1)S(1)} all-to-all(bf16[8,4,2048]{2,1,0:T(4,128)(2,1)S(1)} %shard_map.168), channel_id=1, replica_groups={{0,12,4,8,3,15,7,11},{1,13,5,9,2,14,6,10},{16,28,20,24,19,31,23,27},{17..., dimensions={0} | all-to-all | bytes 262144 | tf_op jit(solution)/shard_map/all_to_all | solution.py:56
  16.3 0.8 %shard_map.169 = bf16[8,2,4,512]{3,2,1,0:T(4,128)(2,1)S(1)} custom-call(bf16[8,4,2048]{2,1,0:T(4,128)(2,1)S(1)} %all_to_all.25.all_ref.tokens_ref, f32[1,2048]{1,0:T(1,128)S(1)} %bitcast.8, bf16[2048,128]{1,0:T(8,128)(2,1)S(1)} %copy-done.1, bf16[2048,128]{1,0:T(8,128)(2,1)S(1)} %collective-permute-done.1.refs_1_, bf16[2048,128]{1,0:T(8,128)(2,1)S(1)} %copy-done.2, ...), custom_call_target="tpu_custom_call" | custom-call | tf_op jit(solution)/shard_map/pallas_call | solution.py:24
  17.1 8.5 %all_to_all.26 = bf16[8,2,4,512]{3,2,1,0:T(4,128)(2,1)S(1)} all-to-all(bf16[8,2,4,512]{3,2,1,0:T(4,128)(2,1)S(1)} %shard_map.169), channel_id=1, replica_groups={{0,12,4,8,3,15,7,11},{1,13,5,9,2,14,6,10},{16,28,20,24,19,31,23,27},{17..., dimensions={0} | all-to-all | bytes 131072 | tf_op jit(solution)/shard_map/all_to_all | solution.py:56
  25.7 0.9 %shard_map.170 = (bf16[8,4,2048]{2,1,0:T(4,128)(2,1)S(1)}, f32[3,64,128]{2,1,0:T(8,128)S(1)}) custom-call(bf16[16,4,512]{2,1,0:T(4,128)(2,1)S(1)} %bitcast.7, f32[4,16,128,128]{3,2,1,0:T(8,128)S(1)} %copy-done, f32[16,128]{1,0:T(8,128)S(1)} %bitcast.9, f32[1,128]{1,0:T(1,128)S(1)} %bitcast.12), custom_call_target="tpu_custom_call" | custom-call | tf_op jit(solution)/shard_map/pallas_call | solution.py:24
  26.6 8.7 %all_to_all.27.all_ref = bf16[8,4,2048]{2,1,0:T(4,128)(2,1)S(1)} all-to-all(bf16[8,4,2048]{2,1,0:T(4,128)(2,1)S(1)} %get-tuple-element.12), channel_id=1, replica_groups={{0,12,4,8,3,15,7,11},{1,13,5,9,2,14,6,10},{16,28,20,24,19,31,23,27},{17..., dimensions={0} | all-to-all | bytes 262144 | tf_op jit(solution)/shard_map/all_to_all | solution.py:56
  35.3 0.3 shard_map.171
  35.6 9.3 %all_to_all.28.mixer_ref = bf16[8,2,32,128]{3,2,1,0:T(8,128)(2,1)S(1)} all-to-all(bf16[8,2,32,128]{3,2,1,0:T(8,128)(2,1)S(1)} %shard_map.171), channel_id=1, replica_groups={{0,12,4,8,3,15,7,11},{1,13,5,9,2,14,6,10},{16,28,20,24,19,31,23,27},{17..., dimensions={0} | all-to-all | bytes 262144 | tf_op jit(solution)/shard_map/all_to_all | solution.py:56
  45.0 0.2 shard_map.172
  45.2 1.0 %collective-permute-start.5 = (bf16[32,2048]{1,0:T(8,128)(2,1)S(1)}, bf16[32,2048]{1,0:T(8,128)(2,1)S(1)}, u32[]{:S(2)}, u32[]{:S(2)}) collective-permute-start(bf16[32,2048]{1,0:T(8,128)(2,1)S(1)} %get-tuple-element.15.mine_ref), channel_id=1, source_target_pairs={{0,1},{1,0},{2,3},{3,2},{4,5},{5,4},{6,7},{7,6},{8,9},{9,8},{10,11... | collective-permute-start | bytes 393224 | tf_op jit(solution)/shard_map/ppermute | solution.py:60
  46.2 1.0 %collective-permute-done.5.other_ref = bf16[32,2048]{1,0:T(8,128)(2,1)S(1)} collective-permute-done((bf16[32,2048]{1,0:T(8,128)(2,1)S(1)}, bf16[32,2048]{1,0:T(8,128)(2,1)S(1)}, u32[]{:S(2)}, u32[]{:S(2)}) %collective-permute-start.5) | collective-permute-done | bytes 131104 | tf_op jit(solution)/shard_map/ppermute | solution.py:60
  47.2 0.0 copy-start.9
  47.2 0.0 copy-start.11
  47.2 4.8 %experts.1 = (f32[8,4,2048]{2,1,0:T(4,128)S(1)}, bf16[8,4,2048]{2,1,0:T(4,128)(2,1)S(1)}, f32[4,16,128,128]{3,2,1,0:T(8,128)}) custom-call(bf16[32,2048]{1,0:T(8,128)(2,1)S(1)} %get-tuple-element.15.mine_ref, bf16[32,2048]{1,0:T(8,128)(2,1)S(1)} %collective-permute-done.5.other_ref, bf16[2048,1792]{1,0:T(8,128)(2,1)S(1)} %bitcast.15, ...), custom_call_target="tpu_custom_call" | custom-call | flops 10000000000 | tf_op jit(solution)/shard_map/experts/pallas_call | solution.py:319
  52.0 0.4 collective-permute-start.6
  52.4 1.0 %collective-permute-done.6.came_ref = bf16[8,4,2048]{2,1,0:T(4,128)(2,1)S(1)} collective-permute-done((bf16[8,4,2048]{2,1,0:T(4,128)(2,1)S(1)}, bf16[8,4,2048]{2,1,0:T(4,128)(2,1)S(1)}, u32[]{:S(2)}, u32[]{:S(2)}) %collective-permute-start.6) | collective-permute-done | bytes 131104 | tf_op jit(solution)/shard_map/ppermute | solution.py:60
  53.4 0.1 shard_map.173
  53.5 8.8 %all_to_all.29.returned_ref = bf16[8,4,2048]{2,1,0:T(4,128)(2,1)S(1)} all-to-all(bf16[8,4,2048]{2,1,0:T(4,128)(2,1)S(1)} %shard_map.173), channel_id=1, replica_groups={{0,12,4,8,3,15,7,11},{1,13,5,9,2,14,6,10},{16,28,20,24,19,31,23,27},{17..., dimensions={0} | all-to-all | bytes 262144 | tf_op jit(solution)/shard_map/all_to_all | solution.py:56
  62.3 0.8 %shard_map.174 = bf16[4,2048]{1,0:T(4,128)(2,1)} custom-call(f32[8,4,2048]{2,1,0:T(4,128)S(1)} %get-tuple-element.14.middle_ref, bf16[8,4,2048]{2,1,0:T(4,128)(2,1)S(1)} %all_to_all.29.returned_ref, s32[2,4]{1,0:T(2,128)S(1)} %bitcast.11, bf16[2,4]{1,0:T(2,128)(2,1)S(1)} %bitcast.13), custom_call_target="tpu_custom_call" | custom-call | tf_op jit(solution)/shard_map/pallas_call | solution.py:24
  (37 shorter events, 0.1 us)
Async XLA Ops:
  0.6 1.6 %copy-start.12 = (bf16[4,2048]{1,0:T(4,128)(2,1)S(1)}, bf16[4,2048]{1,0:T(4,128)(2,1)}, u32[]{:S(2)}) copy-start(bf16[4,2048]{1,0:T(4,128)(2,1)} %rows_ref.1) | copy-start | bytes 49156
  0.6 15.6 %collective-permute-start.1 = (bf16[2048,128]{1,0:T(8,128)(2,1)}, bf16[2048,128]{1,0:T(8,128)(2,1)S(1)}, u32[]{:S(2)}, u32[]{:S(2)}) collective-permute-start(bf16[2048,128]{1,0:T(8,128)(2,1)} %refs_0_.1), channel_id=1, source_target_pairs={{0,1},{1,0},{2,3},{3,2},{4,5},{5,4},{6,7},{7,6},{8,9},{9,8},{10,11... | collective-permute-start | bytes 1572872 | tf_op jit(solution)/shard_map/ppermute | solution.py:60
  1.2 15.0 %collective-permute-start.2 = (bf16[2048,128]{1,0:T(8,128)(2,1)}, bf16[2048,128]{1,0:T(8,128)(2,1)S(1)}, u32[]{:S(2)}, u32[]{:S(2)}) collective-permute-start(bf16[2048,128]{1,0:T(8,128)(2,1)} %refs_2_.1), channel_id=1, source_target_pairs={{0,1},{1,0},{2,3},{3,2},{4,5},{5,4},{6,7},{7,6},{8,9},{9,8},{10,11... | collective-permute-start | bytes 1572872 | tf_op jit(solution)/shard_map/ppermute | solution.py:60
  1.3 15.0 %collective-permute-start.3 = (bf16[2048,128]{1,0:T(8,128)(2,1)}, bf16[2048,128]{1,0:T(8,128)(2,1)S(1)}, u32[]{:S(2)}, u32[]{:S(2)}) collective-permute-start(bf16[2048,128]{1,0:T(8,128)(2,1)} %refs_4_.1), channel_id=1, source_target_pairs={{0,1},{1,0},{2,3},{3,2},{4,5},{5,4},{6,7},{7,6},{8,9},{9,8},{10,11... | collective-permute-start | bytes 1572872 | tf_op jit(solution)/shard_map/ppermute | solution.py:60
  1.7 14.5 %collective-permute-start.4 = (bf16[2048,128]{1,0:T(8,128)(2,1)}, bf16[2048,128]{1,0:T(8,128)(2,1)S(1)}, u32[]{:S(2)}, u32[]{:S(2)}) collective-permute-start(bf16[2048,128]{1,0:T(8,128)(2,1)} %refs_6_.1), channel_id=1, source_target_pairs={{0,1},{1,0},{2,3},{3,2},{4,5},{5,4},{6,7},{7,6},{8,9},{9,8},{10,11... | collective-permute-start | bytes 1572872 | tf_op jit(solution)/shard_map/ppermute | solution.py:60
  1.8 14.4 %collective-permute-start = (bf16[2048,128]{1,0:T(8,128)(2,1)}, bf16[2048,128]{1,0:T(8,128)(2,1)S(1)}, u32[]{:S(2)}, u32[]{:S(2)}) collective-permute-start(bf16[2048,128]{1,0:T(8,128)(2,1)} %own_ref.1), channel_id=1, source_target_pairs={{0,1},{1,0},{2,3},{3,2},{4,5},{5,4},{6,7},{7,6},{8,9},{9,8},{10,11... | collective-permute-start | bytes 1572872 | tf_op jit(solution)/shard_map/ppermute | solution.py:60
  2.2 44.9 %slice-start = ((s8[7340032]{0:T(1024)(128)(4,1)}), s8[4194304]{0:T(1024)(128)(4,1)S(1)}, s32[]{:S(2)}) async-start(s8[7340032]{0:T(1024)(128)(4,1)} %bitcast.14), calls=%async_computation.5 | async-start | bytes 8388608
  2.2 44.9 %slice-start.2 = ((s8[7340032]{0:T(1024)(128)(4,1)}), s8[4194304]{0:T(1024)(128)(4,1)S(1)}, s32[]{:S(2)}) async-start(s8[7340032]{0:T(1024)(128)(4,1)} %bitcast.16), calls=%async_computation.7 | async-start | bytes 8388608
  2.2 44.9 %slice-start.4 = ((s8[7340032]{0:T(1024)(128)(4,1)}), s8[4194304]{0:T(1024)(128)(4,1)S(1)}, s32[]{:S(2)}) async-start(s8[7340032]{0:T(1024)(128)(4,1)} %bitcast.18), calls=%async_computation.9 | async-start | bytes 8388608
  2.2 14.0 %copy-start.1 = (bf16[2048,128]{1,0:T(8,128)(2,1)S(1)}, bf16[2048,128]{1,0:T(8,128)(2,1)}, u32[]{:S(2)}) copy-start(bf16[2048,128]{1,0:T(8,128)(2,1)} %refs_0_.1) | copy-start | bytes 1572868
  2.3 14.0 %copy-start.2 = (bf16[2048,128]{1,0:T(8,128)(2,1)S(1)}, bf16[2048,128]{1,0:T(8,128)(2,1)}, u32[]{:S(2)}) copy-start(bf16[2048,128]{1,0:T(8,128)(2,1)} %refs_2_.1) | copy-start | bytes 1572868
  2.3 14.0 %copy-start.3 = (bf16[2048,128]{1,0:T(8,128)(2,1)S(1)}, bf16[2048,128]{1,0:T(8,128)(2,1)}, u32[]{:S(2)}) copy-start(bf16[2048,128]{1,0:T(8,128)(2,1)} %refs_4_.1) | copy-start | bytes 1572868
  2.3 14.0 %copy-start.4 = (bf16[2048,128]{1,0:T(8,128)(2,1)S(1)}, bf16[2048,128]{1,0:T(8,128)(2,1)}, u32[]{:S(2)}) copy-start(bf16[2048,128]{1,0:T(8,128)(2,1)} %refs_6_.1) | copy-start | bytes 1572868
  2.3 14.0 %copy-start.6 = (f32[2048]{0:T(1024)S(1)}, f32[2048]{0:T(1024)}, u32[]{:S(2)}) copy-start(f32[2048]{0:T(1024)} %param.20) | copy-start | bytes 24580
  2.3 23.4 %copy-start.7 = (f32[2048]{0:T(1024)S(1)}, f32[2048]{0:T(1024)}, u32[]{:S(2)}) copy-start(f32[2048]{0:T(1024)} %param.25) | copy-start | bytes 24580
  2.3 23.4 %copy-start.10 = (f32[128]{0:T(128)S(1)}, f32[128]{0:T(128)}, u32[]{:S(2)}) copy-start(f32[128]{0:T(128)} %param.26) | copy-start | bytes 1540
  2.3 44.8 %slice-start.1 = ((s8[7340032]{0:T(1024)(128)(4,1)}), s8[3145728]{0:T(1024)(128)(4,1)S(1)}, s32[]{:S(2)}) async-start(s8[7340032]{0:T(1024)(128)(4,1)} %bitcast.14), calls=%async_computation.6 | async-start | bytes 6291456
  2.3 44.8 %slice-start.3 = ((s8[7340032]{0:T(1024)(128)(4,1)}), s8[3145728]{0:T(1024)(128)(4,1)S(1)}, s32[]{:S(2)}) async-start(s8[7340032]{0:T(1024)(128)(4,1)} %bitcast.16), calls=%async_computation.8 | async-start | bytes 6291456
  2.4 44.8 %slice-start.5 = ((s8[7340032]{0:T(1024)(128)(4,1)}), s8[3145728]{0:T(1024)(128)(4,1)S(1)}, s32[]{:S(2)}) async-start(s8[7340032]{0:T(1024)(128)(4,1)} %bitcast.18), calls=%async_computation.10 | async-start | bytes 6291456
  2.4 23.3 %copy-start = (f32[4,16,128,128]{3,2,1,0:T(8,128)S(1)}, f32[4,16,128,128]{3,2,1,0:T(8,128)}, u32[]{:S(2)}) copy-start(f32[4,16,128,128]{3,2,1,0:T(8,128)} %state_ref.3) | copy-start | bytes 12582916
  2.4 32.9 %copy-start.5 = (bf16[2048,128]{1,0:T(8,128)(2,1)S(1)}, bf16[2048,128]{1,0:T(8,128)(2,1)}, u32[]{:S(2)}) copy-start(bf16[2048,128]{1,0:T(8,128)(2,1)} %own_ref.1) | copy-start | bytes 1572868
  2.4 42.6 %copy-start.8 = (f32[2048]{0:T(1024)S(1)}, f32[2048]{0:T(1024)}, u32[]{:S(2)}) copy-start(f32[2048]{0:T(1024)} %param.28) | copy-start | bytes 24580
  45.2 2.0 %collective-permute-start.5 = (bf16[32,2048]{1,0:T(8,128)(2,1)S(1)}, bf16[32,2048]{1,0:T(8,128)(2,1)S(1)}, u32[]{:S(2)}, u32[]{:S(2)}) collective-permute-start(bf16[32,2048]{1,0:T(8,128)(2,1)S(1)} %get-tuple-element.15.mine_ref), channel_id=1, source_target_pairs={{0,1},{1,0},{2,3},{3,2},{4,5},{5,4},{6,7},{7,6},{8,9},{9,8},{10,11... | collective-permute-start | bytes 393224 | tf_op jit(solution)/shard_map/ppermute | solution.py:60
  47.2 15.1 %copy-start.9 = (s32[4,2]{0,1:T(2,128)S(1)}, s32[4,2]{0,1:T(2,128)}, u32[]{:S(2)}) copy-start(s32[4,2]{0,1:T(2,128)} %param.18) | copy-start | bytes 100
  47.2 15.1 %copy-start.11 = (bf16[4,2]{0,1:T(2,128)(2,1)S(1)}, bf16[4,2]{0,1:T(2,128)(2,1)}, u32[]{:S(2)}) copy-start(bf16[4,2]{0,1:T(2,128)(2,1)} %param.19) | copy-start | bytes 52
  52.0 1.4 %collective-permute-start.6 = (bf16[8,4,2048]{2,1,0:T(4,128)(2,1)S(1)}, bf16[8,4,2048]{2,1,0:T(4,128)(2,1)S(1)}, u32[]{:S(2)}, u32[]{:S(2)}) collective-permute-start(bf16[8,4,2048]{2,1,0:T(4,128)(2,1)S(1)} %get-tuple-element.18), channel_id=1, source_target_pairs={{0,1},{1,0},{2,3},{3,2},{4,5},{5,4},{6,7},{7,6},{8,9},{9,8},{10,11... | collective-permute-start | bytes 393224 | tf_op jit(solution)/shard_map/ppermute | solution.py:60

commit v5 on v4

--- a/solution.py
+++ b/solution.py
@@ -39,13 +39,15 @@
 def chip_order():
     half = lax.axis_size("chip") // 2
     inward = [i // 2 if i % 2 == 0 else half - 1 - i // 2 for i in range(half)]
-    return [2 * i + odd for odd in range(2) for i in inward]
+    return [2 * z + (lap ^ ((i ^ (i >> 1)) & 1)) for lap in range(2) for i, z in enumerate(inward)]
 
 
 def my_place():
-    chip, half = lax.axis_index("chip"), lax.axis_size("chip") // 2
-    i = chip // 2
-    return (chip % 2) * half + jnp.where(2 * i < half, 2 * i, 2 * (half - 1 - i) + 1)
+    chip = lax.axis_index("chip")
+    place = jnp.int32(0)
+    for i, other in enumerate(chip_order()):
+        place = jnp.where(chip == other, i, place)
+    return place
 
 
 def lines():

time: 63.8 us -> 63.7 us (level)
  no operation moved by 1% of the time
where the time goes in v5:
time: 63.7 us; the launch traced here: 63 us
  blocking collectives  49 us (77%)
  Pallas kernels  7.8 us (12%)
  starting transfers between devices  3.08 us (5%)
  waiting for transfers between devices  1.99 us (3%)
  between operations  0.93 us (1%)
    all_to_all x5, blocking collectives, exchange(): lax.all_to_all(chunks, AXES, split_axis=0, concat_axis=0, axis_index_grou...  49 us
    pallas_call x1, Pallas kernels, body(): pl.pallas_call(expert_body, out_shape=[shape((chips, rows, width), f32),...  4.77 us
    ppermute x7, starting transfers between devices, swap(): return lax.ppermute(values, 'core', [(0, 1), (1, 0)])  3.08 us
    pallas_call x8, Pallas kernels, call(): pl.pallas_call(body, out_shape=outs, in_specs=[pl.BlockSpec(memory_space=...  3.03 us
    ppermute x7, waiting for transfers between devices, swap(): return lax.ppermute(values, 'core', [(0, 1), (1, 0)])  1.99 us
  transfers between devices with their start and end apart: 7, of which 2 were waited for; matrix products, arithmetic and copies ran while one was open for 0% of the time, Pallas kernels for 0%

profile of v5, /device:TPU:0, one launch (start us, length us, event | category | flops | bytes accessed | tf_op | source)
XLA Modules:
  0.0 63.0 jit_solution(13600618461353216007)
XLA Ops:
  0.6 0.6 collective-permute-start.1
  1.2 0.1 collective-permute-start.2
  1.3 0.4 collective-permute-start.3
  1.7 0.1 collective-permute-start.4
  1.8 0.4 collective-permute-start
  2.2 0.0 copy-start.1
  2.3 0.0 copy-start.2
  2.3 0.0 copy-start.3
  2.3 0.0 copy-start.6
  2.3 0.0 copy-start.7
  2.3 0.0 slice-start.1
  2.3 0.0 slice-start.3
  2.4 0.0 slice-start.5
  2.4 0.0 copy-start
  2.4 0.0 copy-start.5
  2.4 13.8 %all_to_all.25.all_ref.tokens_ref = bf16[8,4,2048]{2,1,0:T(4,128)(2,1)S(1)} all-to-all(bf16[8,4,2048]{2,1,0:T(4,128)(2,1)S(1)} %shard_map.168), channel_id=1, replica_groups={{0,15,7,8,3,12,4,11},{1,14,6,9,2,13,5,10},{16,31,23,24,19,28,20,27},{17..., dimensions={0} | all-to-all | bytes 262144 | tf_op jit(solution)/shard_map/all_to_all | solution.py:58
  16.3 0.8 %shard_map.169 = bf16[8,2,4,512]{3,2,1,0:T(4,128)(2,1)S(1)} custom-call(bf16[8,4,2048]{2,1,0:T(4,128)(2,1)S(1)} %all_to_all.25.all_ref.tokens_ref, f32[1,2048]{1,0:T(1,128)S(1)} %bitcast.8, bf16[2048,128]{1,0:T(8,128)(2,1)S(1)} %copy-done.1, bf16[2048,128]{1,0:T(8,128)(2,1)S(1)} %collective-permute-done.1.refs_1_, bf16[2048,128]{1,0:T(8,128)(2,1)S(1)} %copy-done.2, ...), custom_call_target="tpu_custom_call" | custom-call | tf_op jit(solution)/shard_map/pallas_call | solution.py:24
  17.1 8.5 %all_to_all.26 = bf16[8,2,4,512]{3,2,1,0:T(4,128)(2,1)S(1)} all-to-all(bf16[8,2,4,512]{3,2,1,0:T(4,128)(2,1)S(1)} %shard_map.169), channel_id=1, replica_groups={{0,15,7,8,3,12,4,11},{1,14,6,9,2,13,5,10},{16,31,23,24,19,28,20,27},{17..., dimensions={0} | all-to-all | bytes 131072 | tf_op jit(solution)/shard_map/all_to_all | solution.py:58
  25.7 0.9 %shard_map.170 = (bf16[8,4,2048]{2,1,0:T(4,128)(2,1)S(1)}, f32[3,64,128]{2,1,0:T(8,128)S(1)}) custom-call(bf16[16,4,512]{2,1,0:T(4,128)(2,1)S(1)} %bitcast.7, f32[4,16,128,128]{3,2,1,0:T(8,128)S(1)} %copy-done, f32[16,128]{1,0:T(8,128)S(1)} %bitcast.9, f32[1,128]{1,0:T(1,128)S(1)} %bitcast.12), custom_call_target="tpu_custom_call" | custom-call | tf_op jit(solution)/shard_map/pallas_call | solution.py:24
  26.6 8.7 %all_to_all.27.all_ref = bf16[8,4,2048]{2,1,0:T(4,128)(2,1)S(1)} all-to-all(bf16[8,4,2048]{2,1,0:T(4,128)(2,1)S(1)} %get-tuple-element.12), channel_id=1, replica_groups={{0,15,7,8,3,12,4,11},{1,14,6,9,2,13,5,10},{16,31,23,24,19,28,20,27},{17..., dimensions={0} | all-to-all | bytes 262144 | tf_op jit(solution)/shard_map/all_to_all | solution.py:58
  35.2 0.3 shard_map.171
  35.6 9.3 %all_to_all.28.mixer_ref = bf16[8,2,32,128]{3,2,1,0:T(8,128)(2,1)S(1)} all-to-all(bf16[8,2,32,128]{3,2,1,0:T(8,128)(2,1)S(1)} %shard_map.171), channel_id=1, replica_groups={{0,15,7,8,3,12,4,11},{1,14,6,9,2,13,5,10},{16,31,23,24,19,28,20,27},{17..., dimensions={0} | all-to-all | bytes 262144 | tf_op jit(solution)/shard_map/all_to_all | solution.py:58
  44.9 0.2 shard_map.172
  45.0 1.1 %collective-permute-start.5 = (bf16[32,2048]{1,0:T(8,128)(2,1)S(1)}, bf16[32,2048]{1,0:T(8,128)(2,1)S(1)}, u32[]{:S(2)}, u32[]{:S(2)}) collective-permute-start(bf16[32,2048]{1,0:T(8,128)(2,1)S(1)} %get-tuple-element.15.mine_ref), channel_id=1, source_target_pairs={{0,1},{1,0},{2,3},{3,2},{4,5},{5,4},{6,7},{7,6},{8,9},{9,8},{10,11... | collective-permute-start | bytes 393224 | tf_op jit(solution)/shard_map/ppermute | solution.py:62
  46.1 1.0 %collective-permute-done.5.other_ref = bf16[32,2048]{1,0:T(8,128)(2,1)S(1)} collective-permute-done((bf16[32,2048]{1,0:T(8,128)(2,1)S(1)}, bf16[32,2048]{1,0:T(8,128)(2,1)S(1)}, u32[]{:S(2)}, u32[]{:S(2)}) %collective-permute-start.5) | collective-permute-done | bytes 131104 | tf_op jit(solution)/shard_map/ppermute | solution.py:62
  47.2 0.0 copy-start.11
  47.2 4.8 %experts.1 = (f32[8,4,2048]{2,1,0:T(4,128)S(1)}, bf16[8,4,2048]{2,1,0:T(4,128)(2,1)S(1)}, f32[4,16,128,128]{3,2,1,0:T(8,128)}) custom-call(bf16[32,2048]{1,0:T(8,128)(2,1)S(1)} %get-tuple-element.15.mine_ref, bf16[32,2048]{1,0:T(8,128)(2,1)S(1)} %collective-permute-done.5.other_ref, bf16[2048,1792]{1,0:T(8,128)(2,1)S(1)} %bitcast.15, ...), custom_call_target="tpu_custom_call" | custom-call | flops 10000000000 | tf_op jit(solution)/shard_map/experts/pallas_call | solution.py:321
  51.9 0.4 collective-permute-start.6
  52.4 1.0 %collective-permute-done.6.came_ref = bf16[8,4,2048]{2,1,0:T(4,128)(2,1)S(1)} collective-permute-done((bf16[8,4,2048]{2,1,0:T(4,128)(2,1)S(1)}, bf16[8,4,2048]{2,1,0:T(4,128)(2,1)S(1)}, u32[]{:S(2)}, u32[]{:S(2)}) %collective-permute-start.6) | collective-permute-done | bytes 131104 | tf_op jit(solution)/shard_map/ppermute | solution.py:62
  53.4 0.1 shard_map.173
  53.4 8.7 %all_to_all.29.returned_ref = bf16[8,4,2048]{2,1,0:T(4,128)(2,1)S(1)} all-to-all(bf16[8,4,2048]{2,1,0:T(4,128)(2,1)S(1)} %shard_map.173), channel_id=1, replica_groups={{0,15,7,8,3,12,4,11},{1,14,6,9,2,13,5,10},{16,31,23,24,19,28,20,27},{17..., dimensions={0} | all-to-all | bytes 262144 | tf_op jit(solution)/shard_map/all_to_all | solution.py:58
  62.2 0.8 %shard_map.174 = bf16[4,2048]{1,0:T(4,128)(2,1)} custom-call(f32[8,4,2048]{2,1,0:T(4,128)S(1)} %get-tuple-element.14.middle_ref, bf16[8,4,2048]{2,1,0:T(4,128)(2,1)S(1)} %all_to_all.29.returned_ref, s32[2,4]{1,0:T(2,128)S(1)} %bitcast.11, bf16[2,4]{1,0:T(2,128)(2,1)S(1)} %bitcast.13), custom_call_target="tpu_custom_call" | custom-call | tf_op jit(solution)/shard_map/pallas_call | solution.py:24
  (37 shorter events, 0.1 us)
Async XLA Ops:
  0.6 1.6 %copy-start.12 = (bf16[4,2048]{1,0:T(4,128)(2,1)S(1)}, bf16[4,2048]{1,0:T(4,128)(2,1)}, u32[]{:S(2)}) copy-start(bf16[4,2048]{1,0:T(4,128)(2,1)} %rows_ref.1) | copy-start | bytes 49156
  0.6 15.6 %collective-permute-start.1 = (bf16[2048,128]{1,0:T(8,128)(2,1)}, bf16[2048,128]{1,0:T(8,128)(2,1)S(1)}, u32[]{:S(2)}, u32[]{:S(2)}) collective-permute-start(bf16[2048,128]{1,0:T(8,128)(2,1)} %refs_0_.1), channel_id=1, source_target_pairs={{0,1},{1,0},{2,3},{3,2},{4,5},{5,4},{6,7},{7,6},{8,9},{9,8},{10,11... | collective-permute-start | bytes 1572872 | tf_op jit(solution)/shard_map/ppermute | solution.py:62
  1.2 15.0 %collective-permute-start.2 = (bf16[2048,128]{1,0:T(8,128)(2,1)}, bf16[2048,128]{1,0:T(8,128)(2,1)S(1)}, u32[]{:S(2)}, u32[]{:S(2)}) collective-permute-start(bf16[2048,128]{1,0:T(8,128)(2,1)} %refs_2_.1), channel_id=1, source_target_pairs={{0,1},{1,0},{2,3},{3,2},{4,5},{5,4},{6,7},{7,6},{8,9},{9,8},{10,11... | collective-permute-start | bytes 1572872 | tf_op jit(solution)/shard_map/ppermute | solution.py:62
  1.3 15.0 %collective-permute-start.3 = (bf16[2048,128]{1,0:T(8,128)(2,1)}, bf16[2048,128]{1,0:T(8,128)(2,1)S(1)}, u32[]{:S(2)}, u32[]{:S(2)}) collective-permute-start(bf16[2048,128]{1,0:T(8,128)(2,1)} %refs_4_.1), channel_id=1, source_target_pairs={{0,1},{1,0},{2,3},{3,2},{4,5},{5,4},{6,7},{7,6},{8,9},{9,8},{10,11... | collective-permute-start | bytes 1572872 | tf_op jit(solution)/shard_map/ppermute | solution.py:62
  1.7 14.5 %collective-permute-start.4 = (bf16[2048,128]{1,0:T(8,128)(2,1)}, bf16[2048,128]{1,0:T(8,128)(2,1)S(1)}, u32[]{:S(2)}, u32[]{:S(2)}) collective-permute-start(bf16[2048,128]{1,0:T(8,128)(2,1)} %refs_6_.1), channel_id=1, source_target_pairs={{0,1},{1,0},{2,3},{3,2},{4,5},{5,4},{6,7},{7,6},{8,9},{9,8},{10,11... | collective-permute-start | bytes 1572872 | tf_op jit(solution)/shard_map/ppermute | solution.py:62
  1.8 14.4 %collective-permute-start = (bf16[2048,128]{1,0:T(8,128)(2,1)}, bf16[2048,128]{1,0:T(8,128)(2,1)S(1)}, u32[]{:S(2)}, u32[]{:S(2)}) collective-permute-start(bf16[2048,128]{1,0:T(8,128)(2,1)} %own_ref.1), channel_id=1, source_target_pairs={{0,1},{1,0},{2,3},{3,2},{4,5},{5,4},{6,7},{7,6},{8,9},{9,8},{10,11... | collective-permute-start | bytes 1572872 | tf_op jit(solution)/shard_map/ppermute | solution.py:62
  2.2 44.9 %slice-start = ((s8[7340032]{0:T(1024)(128)(4,1)}), s8[4194304]{0:T(1024)(128)(4,1)S(1)}, s32[]{:S(2)}) async-start(s8[7340032]{0:T(1024)(128)(4,1)} %bitcast.14), calls=%async_computation.5 | async-start | bytes 8388608
  2.2 44.9 %slice-start.2 = ((s8[7340032]{0:T(1024)(128)(4,1)}), s8[4194304]{0:T(1024)(128)(4,1)S(1)}, s32[]{:S(2)}) async-start(s8[7340032]{0:T(1024)(128)(4,1)} %bitcast.16), calls=%async_computation.7 | async-start | bytes 8388608
  2.2 44.9 %slice-start.4 = ((s8[7340032]{0:T(1024)(128)(4,1)}), s8[4194304]{0:T(1024)(128)(4,1)S(1)}, s32[]{:S(2)}) async-start(s8[7340032]{0:T(1024)(128)(4,1)} %bitcast.18), calls=%async_computation.9 | async-start | bytes 8388608
  2.2 14.0 %copy-start.1 = (bf16[2048,128]{1,0:T(8,128)(2,1)S(1)}, bf16[2048,128]{1,0:T(8,128)(2,1)}, u32[]{:S(2)}) copy-start(bf16[2048,128]{1,0:T(8,128)(2,1)} %refs_0_.1) | copy-start | bytes 1572868
  2.3 14.0 %copy-start.2 = (bf16[2048,128]{1,0:T(8,128)(2,1)S(1)}, bf16[2048,128]{1,0:T(8,128)(2,1)}, u32[]{:S(2)}) copy-start(bf16[2048,128]{1,0:T(8,128)(2,1)} %refs_2_.1) | copy-start | bytes 1572868
  2.3 14.0 %copy-start.3 = (bf16[2048,128]{1,0:T(8,128)(2,1)S(1)}, bf16[2048,128]{1,0:T(8,128)(2,1)}, u32[]{:S(2)}) copy-start(bf16[2048,128]{1,0:T(8,128)(2,1)} %refs_4_.1) | copy-start | bytes 1572868
  2.3 14.0 %copy-start.4 = (bf16[2048,128]{1,0:T(8,128)(2,1)S(1)}, bf16[2048,128]{1,0:T(8,128)(2,1)}, u32[]{:S(2)}) copy-start(bf16[2048,128]{1,0:T(8,128)(2,1)} %refs_6_.1) | copy-start | bytes 1572868
  2.3 14.0 %copy-start.6 = (f32[2048]{0:T(1024)S(1)}, f32[2048]{0:T(1024)}, u32[]{:S(2)}) copy-start(f32[2048]{0:T(1024)} %param.20) | copy-start | bytes 24580
  2.3 23.4 %copy-start.7 = (f32[2048]{0:T(1024)S(1)}, f32[2048]{0:T(1024)}, u32[]{:S(2)}) copy-start(f32[2048]{0:T(1024)} %param.25) | copy-start | bytes 24580
  2.3 23.4 %copy-start.10 = (f32[128]{0:T(128)S(1)}, f32[128]{0:T(128)}, u32[]{:S(2)}) copy-start(f32[128]{0:T(128)} %param.26) | copy-start | bytes 1540
  2.3 44.8 %slice-start.1 = ((s8[7340032]{0:T(1024)(128)(4,1)}), s8[3145728]{0:T(1024)(128)(4,1)S(1)}, s32[]{:S(2)}) async-start(s8[7340032]{0:T(1024)(128)(4,1)} %bitcast.14), calls=%async_computation.6 | async-start | bytes 6291456
  2.3 44.8 %slice-start.3 = ((s8[7340032]{0:T(1024)(128)(4,1)}), s8[3145728]{0:T(1024)(128)(4,1)S(1)}, s32[]{:S(2)}) async-start(s8[7340032]{0:T(1024)(128)(4,1)} %bitcast.16), calls=%async_computation.8 | async-start | bytes 6291456
  2.4 44.8 %slice-start.5 = ((s8[7340032]{0:T(1024)(128)(4,1)}), s8[3145728]{0:T(1024)(128)(4,1)S(1)}, s32[]{:S(2)}) async-start(s8[7340032]{0:T(1024)(128)(4,1)} %bitcast.18), calls=%async_computation.10 | async-start | bytes 6291456
  2.4 23.3 %copy-start = (f32[4,16,128,128]{3,2,1,0:T(8,128)S(1)}, f32[4,16,128,128]{3,2,1,0:T(8,128)}, u32[]{:S(2)}) copy-start(f32[4,16,128,128]{3,2,1,0:T(8,128)} %state_ref.3) | copy-start | bytes 12582916
  2.4 32.8 %copy-start.5 = (bf16[2048,128]{1,0:T(8,128)(2,1)S(1)}, bf16[2048,128]{1,0:T(8,128)(2,1)}, u32[]{:S(2)}) copy-start(bf16[2048,128]{1,0:T(8,128)(2,1)} %own_ref.1) | copy-start | bytes 1572868
  2.4 42.4 %copy-start.8 = (f32[2048]{0:T(1024)S(1)}, f32[2048]{0:T(1024)}, u32[]{:S(2)}) copy-start(f32[2048]{0:T(1024)} %param.28) | copy-start | bytes 24580
  45.0 2.1 %collective-permute-start.5 = (bf16[32,2048]{1,0:T(8,128)(2,1)S(1)}, bf16[32,2048]{1,0:T(8,128)(2,1)S(1)}, u32[]{:S(2)}, u32[]{:S(2)}) collective-permute-start(bf16[32,2048]{1,0:T(8,128)(2,1)S(1)} %get-tuple-element.15.mine_ref), channel_id=1, source_target_pairs={{0,1},{1,0},{2,3},{3,2},{4,5},{5,4},{6,7},{7,6},{8,9},{9,8},{10,11... | collective-permute-start | bytes 393224 | tf_op jit(solution)/shard_map/ppermute | solution.py:62
  47.1 15.0 %copy-start.9 = (s32[4,2]{0,1:T(2,128)S(1)}, s32[4,2]{0,1:T(2,128)}, u32[]{:S(2)}) copy-start(s32[4,2]{0,1:T(2,128)} %param.18) | copy-start | bytes 100
  47.2 15.0 %copy-start.11 = (bf16[4,2]{0,1:T(2,128)(2,1)S(1)}, bf16[4,2]{0,1:T(2,128)(2,1)}, u32[]{:S(2)}) copy-start(bf16[4,2]{0,1:T(2,128)(2,1)} %param.19) | copy-start | bytes 52
  51.9 1.4 %collective-permute-start.6 = (bf16[8,4,2048]{2,1,0:T(4,128)(2,1)S(1)}, bf16[8,4,2048]{2,1,0:T(4,128)(2,1)S(1)}, u32[]{:S(2)}, u32[]{:S(2)}) collective-permute-start(bf16[8,4,2048]{2,1,0:T(4,128)(2,1)S(1)} %get-tuple-element.18), channel_id=1, source_target_pairs={{0,1},{1,0},{2,3},{3,2},{4,5},{5,4},{6,7},{7,6},{8,9},{9,8},{10,11... | collective-permute-start | bytes 393224 | tf_op jit(solution)/shard_map/ppermute | solution.py:62
